TPU v7x, 32 devices: a whole 2x2x4 slice. The times are simulated.
32 devices in a mesh: fs: 8 (over z, y), tp: 4 (over x, core).
Axes of the slice: x: 2, y: 2, z: 4, core: 2. Of those that a mesh axis runs over, the one named last changes fastest.
Arguments:
- saved_input: bfloat16 [6144, 2048], P('fs'), may hold values from -6 to 6
- cot_inproj: bfloat16 [6144, 1024], P('fs', 'tp'), may hold values from -0.076171875 to 0.076171875
- cot_outproj: bfloat16 [6144, 1024], P('fs', 'tp'), may hold values from -0.076171875 to 0.076171875
- factor_inproj: bfloat16 [2048, 256], P('fs')
- factor_outproj: bfloat16 [2048, 256], P('fs')
- weight_inproj: float32 [2048, 1024], P('fs', 'tp'), may hold values from -0.125 to 0.125
- weight_outproj: float32 [2048, 1024], P('fs', 'tp'), may hold values from -0.125 to 0.125
- first_inproj: float32 [256, 1024], P('fs', 'tp'), may hold values from -6 to 6
- first_outproj: float32 [256, 1024], P('fs', 'tp'), may hold values from -6 to 6
- second_inproj: float32 [256, 1024], P('fs', 'tp'), may hold values from 0.25 to 4
- second_outproj: float32 [256, 1024], P('fs', 'tp'), may hold values from 0.25 to 4
Outputs:
- update_inproj: float32 [2048, 1024], P('fs', 'tp')
- update_outproj: float32 [2048, 1024], P('fs', 'tp')
- new_inproj: float32 [2048, 1024], P('fs', 'tp')
- new_outproj: float32 [2048, 1024], P('fs', 'tp')
- copy_inproj: bfloat16 [2048, 1024], P(None, 'tp')
- copy_outproj: bfloat16 [2048, 1024], P(None, 'tp')
- first_inproj_new: float32 [256, 1024], P('fs', 'tp')
- first_outproj_new: float32 [256, 1024], P('fs', 'tp')
- second_inproj_new: float32 [256, 1024], P('fs', 'tp')
- second_outproj_new: float32 [256, 1024], P('fs', 'tp')
All inputs are finite; a program needn't handle non-finite values.
Results may differ from a plain program's by a relative error of at most 0.00045.
Values may be sent and summed in bfloat16 or wider, within the bound.
A program may use at most 64 MiB of HBM per device.

v0:
```python
import functools

import jax
import jax.numpy as jnp
from jax import lax
from jax.experimental import pallas as pl
from jax.experimental.pallas import tpu as pltpu
from jax.sharding import PartitionSpec as P


def contract_rows(left, right, precision):
    return lax.dot_general(
        left,
        right,
        (((0,), (0,)), ((), ())),
        precision=precision,
        preferred_element_type=jnp.float32,
    )


def plain_form(
    saved_input,
    cot_inproj,
    cot_outproj,
    factor_inproj,
    factor_outproj,
    weight_inproj,
    weight_outproj,
    first_inproj,
    first_outproj,
    second_inproj,
    second_outproj,
):
    highest = lax.Precision.HIGHEST
    pieces = (
        lax.all_gather(factor_inproj, "fs", axis=0, tiled=True),
        lax.all_gather(factor_outproj, "fs", axis=0, tiled=True),
    )
    mapped_in = jnp.dot(saved_input, pieces[0], preferred_element_type=jnp.float32)
    mapped_out = jnp.dot(saved_input, pieces[1], preferred_element_type=jnp.float32)
    term_in = contract_rows(mapped_in, cot_inproj.astype(jnp.float32), highest)
    term_out = contract_rows(mapped_out, cot_outproj.astype(jnp.float32), highest)
    projected_in, projected_out = (
        lax.psum_scatter(term_in, "fs", scatter_dimension=0, tiled=True),
        lax.psum_scatter(term_out, "fs", scatter_dimension=0, tiled=True),
    )
    first_in_new = 0.8 * first_inproj + 0.2 * projected_in
    first_out_new = 0.8 * first_outproj + 0.2 * projected_out
    second_in_new = 0.9 * second_inproj + 0.1 * projected_in * projected_in
    second_out_new = 0.9 * second_outproj + 0.1 * projected_out * projected_out
    small_in = first_in_new / (jnp.sqrt(second_in_new) + 1e-08)
    small_out = first_out_new / (jnp.sqrt(second_out_new) + 1e-08)
    wide_in = factor_inproj.astype(jnp.float32)
    wide_out = factor_outproj.astype(jnp.float32)
    pieces = (
        lax.all_gather(small_in, "fs", axis=0, tiled=True),
        lax.all_gather(small_out, "fs", axis=0, tiled=True),
    )
    full_in = jnp.dot(wide_in, pieces[0], precision=highest)
    full_out = jnp.dot(wide_out, pieces[1], precision=highest)
    square_in, square_out = lax.psum(
        (jnp.sum(full_in * full_in), jnp.sum(full_out * full_out)), ("fs", "tp")
    )
    entries = float(full_in.shape[0] * full_in.shape[1] * lax.axis_size("fs") * lax.axis_size("tp"))
    update_in = full_in / jnp.sqrt(square_in / entries + 1e-06)
    update_out = full_out / jnp.sqrt(square_out / entries + 1e-06)
    fresh_in = weight_inproj - 0.02 * update_in
    fresh_out = weight_outproj - 0.02 * update_out
    copy_in, copy_out = (
        lax.all_gather(fresh_in.astype(jnp.bfloat16), "fs", axis=0, tiled=True),
        lax.all_gather(fresh_out.astype(jnp.bfloat16), "fs", axis=0, tiled=True),
    )
    return (
        update_in,
        update_out,
        fresh_in,
        fresh_out,
        copy_in,
        copy_out,
        first_in_new,
        first_out_new,
        second_in_new,
        second_out_new,
    )


MESH = pl.DeviceIdType.MESH
F32, BF16 = jnp.float32, jnp.bfloat16


def parts_of(x):
    high = x.astype(BF16)
    rest = x - high.astype(F32)
    middle = rest.astype(BF16)
    return high, middle, (rest - middle.astype(F32)).astype(BF16)


def dot(a, b):
    return jnp.dot(a, b, preferred_element_type=F32)


class Gather:
    def goes_up(self, s):
        z, last = self.z, self.depth - 1
        needed = (z - s >= 0) & (z < last)
        return needed & (z != last - 1) if self.near and s == 0 else needed

    def goes_down(self, s):
        z, last = self.z, self.depth - 1
        needed = (z + s <= last) & (z >= 1)
        return needed & (z != 1) if self.near and s == 0 else needed

    def crosses(self, zi, c):
        sent = jnp.logical_not(self.detour(zi, c))
        return sent & (zi != self.z) if self.near else sent

    def __init__(self, place, chunks, ref_of, sems, near=False):
        self.z, self.y, self.tp, self.depth = place
        self.near = near
        self.chunks, self.ref_of = chunks, ref_of
        self.up_s, self.up_r, self.dn_s, self.dn_r, self.y_s, self.y_r, self.x_s, self.x_r = sems

    def detour(self, zi, c):
        z, last = self.z, self.depth - 1
        if self.depth < 4:
            return z < 0
        end = ((z == 1) & (zi == 0)) | ((z == last - 1) & (zi == last))
        if c >= self.chunks // 2:
            end = end | ((z == 0) & (zi == 1)) | ((z == last) & (zi == last - 1))
        return end

    def copy(self, zi, yi, c, s_sem, r_sem, to_z, to_y):
        ref = self.ref_of(zi * 2 + yi, c)
        return pltpu.make_async_remote_copy(
            src_ref=ref, dst_ref=ref, send_sem=s_sem, recv_sem=r_sem,
            device_id=(to_z * 2 + to_y, self.tp), device_id_type=MESH,
        )

    def up(self, s, c):
        return self.copy(self.z - s, self.y, c, self.up_s.at[s, c], self.up_r.at[s, c], self.z + 1, self.y)

    def down(self, s, c):
        return self.copy(self.z + s, self.y, c, self.dn_s.at[s, c], self.dn_r.at[s, c], self.z - 1, self.y)

    def from_below(self, s, c):
        return self.copy(self.z - 1 - s, self.y, c, self.up_s.at[s, c], self.up_r.at[s, c], self.z, self.y)

    def from_above(self, s, c):
        return self.copy(self.z + 1 + s, self.y, c, self.dn_s.at[s, c], self.dn_r.at[s, c], self.z, self.y)

    def across(self, zi, c):
        return self.copy(zi, self.y, c, self.y_s.at[zi, c], self.y_r.at[zi, c], self.z, 1 - self.y)

    def from_across(self, zi, c):
        return self.copy(zi, 1 - self.y, c, self.y_s.at[zi, c], self.y_r.at[zi, c], self.z, self.y)

    def beside(self, c, to_z):
        return self.copy(self.z, 1 - self.y, c, self.x_s.at[c], self.x_r.at[c], to_z, self.y)

    def from_beside(self, zi, c):
        return self.copy(zi, 1 - self.y, c, self.x_s.at[c], self.x_r.at[c], self.z, self.y)

    def beside_cases(self, c):
        if self.depth < 4:
            return ()
        z, last = self.z, self.depth - 1
        cases = [(z == 0, 1), (z == last, last - 1)]
        if c >= self.chunks // 2:
            cases += [(z == 1, 0), (z == last - 1, last)]
        return cases

    def start(self, c):
        @pl.when(self.goes_up(0))
        def _():
            self.up(0, c).start()

        @pl.when(self.goes_down(0))
        def _():
            self.down(0, c).start()

        if not self.near:
            self.across(self.z, c).start()

    def start_beside(self, c):
        for condition, neighbour in self.beside_cases(c):
            @pl.when(condition)
            def _():
                self.beside(c, neighbour).start()

    def hand_on(self, zi, c):
        @pl.when(jnp.logical_not(self.detour(zi, c)))
        def _():
            self.across(zi, c).start()

    def land(self, zi, c, have):
        gone = self.detour(zi, c)

        @pl.when(gone)
        def _():
            self.from_beside(zi, c).wait_recv()

        @pl.when(jnp.logical_not(gone))
        def _():
            self.from_across(zi, c).wait_recv()

        have(zi * 2 + 1 - self.y, c)

    def relay(self, have=None, after=None):
        have = have or (lambda block, c: None)
        z, depth = self.z, self.depth
        for s in range(1, depth + 1):
            for c in range(self.chunks):
                if s < depth:
                    @pl.when(z - s >= 0)
                    def _():
                        if self.near and s == 1:
                            @pl.when(z != depth - 1)
                            def _():
                                self.from_below(0, c).wait_recv()
                        else:
                            self.from_below(s - 1, c).wait_recv()
                        if s < depth - 1:
                            @pl.when(z + 1 < depth)
                            def _():
                                self.up(s, c).start()
                        self.hand_on(z - s, c)
                        have((z - s) * 2 + self.y, c)

                    @pl.when(z + s < depth)
                    def _():
                        if self.near and s == 1:
                            @pl.when(z != 0)
                            def _():
                                self.from_above(0, c).wait_recv()
                        else:
                            self.from_above(s - 1, c).wait_recv()
                        if s < depth - 1:
                            @pl.when(z >= 1)
                            def _():
                                self.down(s, c).start()
                        self.hand_on(z + s, c)
                        have((z + s) * 2 + self.y, c)

                if s == 1:
                    if not self.near:
                        self.from_across(z, c).wait_recv()
                        self.start_beside(c)
                        have(z * 2 + 1 - self.y, c)
                else:
                    @pl.when(z - (s - 1) >= 0)
                    def _():
                        self.land(z - (s - 1), c, have)

                    @pl.when(z + (s - 1) < depth)
                    def _():
                        self.land(z + (s - 1), c, have)
            if after is not None:
                after(s)

    def finish(self):
        for c in range(self.chunks):
            for s in range(self.depth - 1):
                @pl.when(self.goes_up(s))
                def _():
                    self.up(s, c).wait_send()

                @pl.when(self.goes_down(s))
                def _():
                    self.down(s, c).wait_send()
            for zi in range(self.depth):
                @pl.when(self.crosses(zi, c))
                def _():
                    self.across(zi, c).wait_send()
            for condition, neighbour in self.beside_cases(c):
                @pl.when(condition)
                def _():
                    self.beside(c, neighbour).wait_send()


def gather_sems(depth, chunks):
    dma = pltpu.SemaphoreType.DMA
    return [dma((depth - 1, chunks))] * 4 + [dma((depth, chunks))] * 2 + [dma((chunks,))] * 2


def kernel(
    n, tps, entries,
    saved_hbm, cot_in_hbm, cot_out_hbm, factor_in_hbm, factor_out_hbm, weight_in_hbm, weight_out_hbm,
    first_in_hbm, first_out_hbm, second_in_hbm, second_out_hbm,
    update, fresh, copies, first_new, second_new,
    saved, cots, factors, weights, first, second, mapped, terms, crossed, staged, landed, smalls, squares, early, ahead,
    wy_s, wy_r, wz_s, wz_r, load_sem, pair_s, pair_r, ty_s, ty_r, tz_s, tz_r, sz_s, sz_r, sy_s, sy_r, norm_s, norm_r, *gather_refs,
):
    me, tp = lax.axis_index("fs"), lax.axis_index("tp")
    z, y = me // 2, me % 2
    depth = n // 2
    side = tp % 2
    partner = tp + 1 - 2 * side
    rows = factors.shape[2]
    half = rows // 2
    slim = first.shape[1]
    place = (z, y, tp, depth)

    barrier = pltpu.get_barrier_semaphore()
    for k in range(1, depth):
        pl.semaphore_signal(barrier, inc=1, device_id=((z + k) % depth * 2 + y, tp), device_id_type=MESH)
    pl.semaphore_signal(barrier, inc=1, device_id=(z * 2 + 1 - y, tp), device_id_type=MESH)
    for k in range(1, tps):
        pl.semaphore_signal(barrier, inc=1, device_id=(me, (tp + k) % tps), device_id_type=MESH)

    loads = [
        pltpu.make_async_copy(source, target, load_sem.at[i])
        for i, (source, target) in enumerate((
            (factor_in_hbm, factors.at[0, me]), (factor_out_hbm, factors.at[1, me]),
            (saved_hbm, saved), (cot_in_hbm, cots.at[0]), (cot_out_hbm, cots.at[1]),
            (first_in_hbm, first.at[0]), (first_out_hbm, first.at[1]),
            (second_in_hbm, second.at[0]), (second_out_hbm, second.at[1]),
            (weight_in_hbm, weights.at[0]), (weight_out_hbm, weights.at[1]),
        ))
    ]
    for load in loads:
        load.start()
    loads[0].wait()
    loads[1].wait()
    pl.semaphore_wait(barrier, depth + tps - 1)

    def factor_ref(m, block, c):
        return factors.at[m, block, pl.ds(c * half, half)]

    def hand(m, block, c):
        ref = factor_ref(m, block, c)
        return pltpu.make_async_remote_copy(
            src_ref=ref, dst_ref=ref, send_sem=pair_s.at[block, c], recv_sem=pair_r.at[block, c],
            device_id=(me, partner), device_id_type=MESH,
        )

    gather = Gather(place, 2, lambda block, c: factor_ref(side, block, c), gather_refs[:8])
    gather.start(0)
    gather.start(1)
    loads[2].wait()

    def map_block(block, first_one=False):
        piece = saved[:, pl.ds(pl.multiple_of(block * rows, rows), rows)]
        for m in range(2):
            product = dot(piece, factors[m, block])
            mapped[m] = product if first_one else mapped[m] + product

    def map_handed(block):
        for c in range(2):
            hand(1 - side, block, c).wait_recv()
        map_block(block)

    def map_at(distance):
        if distance == 0:
            map_handed(z * 2 + 1 - y)
            return

        @pl.when(z - distance >= 0)
        def _():
            map_handed((z - distance) * 2 + y)
            map_handed((z - distance) * 2 + 1 - y)

        @pl.when(z + distance < depth)
        def _():
            map_handed((z + distance) * 2 + y)
            map_handed((z + distance) * 2 + 1 - y)

    at_end = (z == 0) | (z == depth - 1)
    inner = jnp.where(z == 0, 1, depth - 2)
    by_end = (z == 1) | (z == depth - 2)
    outer = jnp.where(z == 1, 0, depth - 1)

    def early_cross(m, c):
        return pltpu.make_async_remote_copy(
            src_ref=weights.at[m, pl.ds(c * half, half)], dst_ref=early.at[0, m, pl.ds(c * half, half)],
            send_sem=wy_s.at[m, c], recv_sem=wy_r.at[m, c], device_id=(z * 2 + 1 - y, tp), device_id_type=MESH,
        )

    def early_along(m, c):
        return pltpu.make_async_remote_copy(
            src_ref=weights.at[m, pl.ds(c * half, half)], dst_ref=early.at[1, m, pl.ds(c * half, half)],
            send_sem=wz_s.at[m, c], recv_sem=wz_r.at[m, c], device_id=(outer * 2 + y, tp), device_id_type=MESH,
        )

    def early_along_start(m):
        @pl.when(by_end)
        def _():
            for c in range(2):
                early_along(m, c).start()

    map_block(me, True)
    gather.relay(
        lambda block, c: hand(side, block, c).start(),
        lambda s: map_at(s - 2) if s >= 2 else None,
    )
    for load in loads[3:]:
        load.wait()
    early_cross(0, 0).start()
    early_along_start(0)
    map_at(depth - 1)

    def term_cross(m, zi):
        return pltpu.make_async_remote_copy(
            src_ref=terms.at[m, zi * 2 + 1 - y], dst_ref=crossed.at[m, zi],
            send_sem=ty_s.at[m, zi], recv_sem=ty_r.at[m, zi],
            device_id=(z * 2 + 1 - y, tp), device_id_type=MESH,
        )

    def term_along(m, zi):
        return pltpu.make_async_remote_copy(
            src_ref=staged.at[m, zi], dst_ref=landed.at[m, z], send_sem=tz_s.at[m, zi], recv_sem=tz_r.at[m, z],
            device_id=(zi * 2 + y, tp), device_id_type=MESH,
        )

    def term_from(m, zi):
        return pltpu.make_async_remote_copy(
            src_ref=staged.at[m, z], dst_ref=landed.at[m, zi], send_sem=tz_s.at[m, z], recv_sem=tz_r.at[m, zi],
            device_id=(z * 2 + y, tp), device_id_type=MESH,
        )

    order = [k % depth for k in range(1, depth + 1)]
    for m in range(2):
        high, middle, low = parts_of(mapped[m].T)
        term = dot(high, cots[m]) + (dot(middle, cots[m]) + dot(low, cots[m]))
        terms[m] = term.reshape(n, slim, term.shape[1])
        for k in order:
            term_cross(m, (z + k) % depth).start()
    for m in range(2):
        for k in order:
            zi = (z + k) % depth
            term_cross(m, zi).wait_recv()
            staged[m, zi] = terms[m, zi * 2 + y] + crossed[m, zi]
            if k:
                term_along(m, zi).start()

    early_cross(0, 1).start()

    def small_along(m, zi):
        ref = smalls.at[m, me]
        return pltpu.make_async_remote_copy(
            src_ref=ref, dst_ref=ref, send_sem=sz_s.at[m, zi], recv_sem=sz_r.at[m, z],
            device_id=(zi * 2 + y, tp), device_id_type=MESH,
        )

    def small_from(m, zi):
        ref = smalls.at[m, zi * 2 + y]
        return pltpu.make_async_remote_copy(
            src_ref=ref, dst_ref=ref, send_sem=sz_s.at[m, zi], recv_sem=sz_r.at[m, zi],
            device_id=(z * 2 + y, tp), device_id_type=MESH,
        )

    def small_cross(m, zi, column):
        ref = smalls.at[m, zi * 2 + column]
        return pltpu.make_async_remote_copy(
            src_ref=ref, dst_ref=ref, send_sem=sy_s.at[m, zi], recv_sem=sy_r.at[m, zi],
            device_id=(z * 2 + 1 - y, tp), device_id_type=MESH,
        )

    for m in range(2):
        here = staged[m, z]
        for k in range(1, depth):
            term_from(m, (z + k) % depth).wait_recv()
            here = here + landed[m, (z + k) % depth]
        first_m = 0.8 * first[m] + 0.2 * here
        second_m = 0.9 * second[m] + 0.1 * here * here
        first_new[m] = first_m
        second_new[m] = second_m
        smalls[m, me] = first_m / (jnp.sqrt(second_m) + 1e-08)
        for k in range(1, depth):
            small_along(m, (z + k) % depth).start()
        small_cross(m, z, y).start()
    for m in range(2):
        for k in range(1, depth):
            zi = (z + k) % depth
            small_from(m, zi).wait_recv()
            small_cross(m, zi, y).start()

    def send_square(m, k):
        return pltpu.make_async_remote_copy(
            src_ref=squares.at[m, tp], dst_ref=squares.at[m, tp], send_sem=norm_s.at[m, k], recv_sem=norm_r.at[m, k],
            device_id=(me, (tp + k) % tps), device_id_type=MESH,
        )

    def recv_square(m, k):
        ref = squares.at[m, (tp + tps - k) % tps]
        return pltpu.make_async_remote_copy(
            src_ref=ref, dst_ref=ref, send_sem=norm_s.at[m, k], recv_sem=norm_r.at[m, k],
            device_id=(me, tp), device_id_type=MESH,
        )

    early_cross(1, 0).start()
    early_cross(1, 1).start()
    early_along_start(1)

    def chunk_ref(block, c):
        return copies.at[c // 2, block, pl.ds(c % 2 * half, half)]

    copy_gather = Gather(place, 4, chunk_ref, gather_refs[8:], near=True)
    beside = z * 2 + 1 - y
    behind = inner * 2 + y
    for m in range(2):
        for k in range(depth):
            small_cross(m, (z + k) % depth, 1 - y).wait_recv()
        high, middle, low = parts_of(smalls[m].reshape(n * slim, smalls.shape[3]))

        def full_of(block):
            factor = factors[m, block]
            return dot(factor, high) + (dot(factor, middle) + dot(factor, low))

        total = None
        for block in range(n):
            full = full_of(block)
            square = jnp.sum((full * full).reshape(rows // 8, 8, full.shape[1]), axis=0)
            total = square if total is None else total + square
        squares[m, tp] = total
        for k in range(1, tps):
            send_square(m, k).start()
        update[m] = full_of(me)
        ahead[0] = full_of(beside)

        @pl.when(at_end)
        def _():
            ahead[1] = full_of(behind)

        for k in range(1, tps):
            recv_square(m, k).wait_recv()
        mean = jnp.sum(jnp.sum(squares[m], axis=0), keepdims=True) / entries
        root = jnp.sqrt(mean + 1e-06)
        new_update = update[m] / root
        new_weight = weights[m] - 0.02 * new_update
        copies[m, me] = new_weight.astype(BF16)
        for c in range(2 * m, 2 * m + 2):
            copy_gather.start(c)
        update[m] = new_update
        fresh[m] = new_weight
        for c in range(2):
            early_cross(m, c).wait_recv()
        copies[m, beside] = (early[0, m] - 0.02 * (ahead[0] / root)).astype(BF16)
        for c in range(2 * m, 2 * m + 2):
            copy_gather.start_beside(c)

        @pl.when(at_end)
        def _():
            for c in range(2):
                early_along(m, c).wait_recv()
            copies[m, behind] = (early[1, m] - 0.02 * (ahead[1] / root)).astype(BF16)

    copy_gather.relay()

    for m in range(2):
        for c in range(2):
            early_cross(m, c).wait_send()

            @pl.when(by_end)
            def _():
                early_along(m, c).wait_send()
    gather.finish()
    copy_gather.finish()
    for k in range(1, n):
        for c in range(2):
            hand(side, (me + k) % n, c).wait_send()
    for m in range(2):
        for k in range(depth):
            zi = (z + k) % depth
            term_cross(m, zi).wait_send()
            small_cross(m, zi, y).wait_send()
            if k:
                term_along(m, zi).wait_send()
                small_along(m, zi).wait_send()
        for k in range(1, tps):
            send_square(m, k).wait_send()


def write_kernel(update, fresh, copies, first_new, second_new, *refs):
    outs, sem = refs[:-1], refs[-1]
    started = []
    for i, source in enumerate((update, fresh, copies, first_new, second_new)):
        for m in range(2):
            copy = pltpu.make_async_copy(source.at[m], outs[2 * i + m], sem.at[2 * i + m])
            copy.start()
            started.append(copy)
    for copy in started:
        copy.wait()


def kernel_form(n, tps, saved_input, cot_inproj, cot_outproj, factor_inproj, *others):
    tokens, wide = saved_input.shape
    columns = cot_inproj.shape[1]
    rows, rank = factor_inproj.shape
    slim = rank // n
    depth = n // 2
    entries = float(wide * columns * tps)
    dma = pltpu.SemaphoreType.DMA
    vmem = pl.BlockSpec(memory_space=pltpu.VMEM)
    anywhere = pl.BlockSpec(memory_space=pl.ANY)
    far = pl.BlockSpec(memory_space=pltpu.HBM)
    shape = jax.ShapeDtypeStruct
    results = pl.pallas_call(
        functools.partial(kernel, n, tps, entries),
        out_shape=(
            shape((2, rows, columns), F32), shape((2, rows, columns), F32),
            shape((2, n, rows, columns), BF16),
            shape((2, slim, columns), F32), shape((2, slim, columns), F32),
        ),
        in_specs=[far] * 11,
        out_specs=[vmem] * 5,
        scratch_shapes=[
            pltpu.VMEM((tokens, wide), BF16),
            pltpu.VMEM((2, tokens, columns), BF16),
            pltpu.VMEM((2, n, rows, rank), BF16),
            pltpu.VMEM((2, rows, columns), F32),
            pltpu.VMEM((2, slim, columns), F32),
            pltpu.VMEM((2, slim, columns), F32),
            pltpu.VMEM((2, tokens, rank), F32),
            pltpu.VMEM((2, n, slim, columns), F32),
            pltpu.VMEM((2, depth, slim, columns), F32),
            pltpu.VMEM((2, depth, slim, columns), F32),
            pltpu.VMEM((2, depth, slim, columns), F32),
            pltpu.VMEM((2, n, slim, columns), F32),
            pltpu.VMEM((2, tps, 8, columns), F32),
            pltpu.VMEM((2, 2, rows, columns), F32),
            pltpu.VMEM((2, rows, columns), F32),
            *[dma((2, 2))] * 4,
            dma((11,)),
            dma((n, 2)), dma((n, 2)),
            *[dma((2, depth))] * 8,
            dma((2, tps)), dma((2, tps)),
            *gather_sems(depth, 2), *gather_sems(depth, 4),
        ],
        compiler_params=pltpu.CompilerParams(collective_id=0, has_side_effects=True, vmem_limit_bytes=40 * 2**20),
    )(*[pltpu.with_memory_space_constraint(x, pltpu.HBM) for x in (saved_input, cot_inproj, cot_outproj, factor_inproj, *others)])
    update, fresh, copies, first_new, second_new = results
    copies = copies.reshape(2, n * rows, columns)
    return pl.pallas_call(
        write_kernel,
        out_shape=(
            *[shape((rows, columns), F32)] * 4, *[shape((n * rows, columns), BF16)] * 2, *[shape((slim, columns), F32)] * 4,
        ),
        in_specs=[anywhere] * 5,
        out_specs=[far] * 10,
        scratch_shapes=[dma((10,))],
        compiler_params=pltpu.CompilerParams(vmem_limit_bytes=2**20),
    )(update, fresh, copies, first_new, second_new)


def on_device(saved_input, cot_inproj, cot_outproj, factor_inproj, *others):
    n, tps = lax.axis_size("fs"), lax.axis_size("tp")
    rows, rank = factor_inproj.shape
    if n % 2 == 0 and n >= 8 and tps % 2 == 0 and rank % (8 * n) == 0 and rows % 128 == 0 and cot_inproj.shape[1] % 128 == 0:
        return kernel_form(n, tps, saved_input, cot_inproj, cot_outproj, factor_inproj, *others)
    return plain_form(saved_input, cot_inproj, cot_outproj, factor_inproj, *others)


def solution(mesh):
    return jax.shard_map(
        on_device,
        mesh=mesh,
        in_specs=(
            P("fs", None),
            P("fs", "tp"),
            P("fs", "tp"),
            P("fs", None),
            P("fs", None),
            P("fs", "tp"),
            P("fs", "tp"),
            P("fs", "tp"),
            P("fs", "tp"),
            P("fs", "tp"),
            P("fs", "tp"),
        ),
        out_specs=(
            P("fs", "tp"),
            P("fs", "tp"),
            P("fs", "tp"),
            P("fs", "tp"),
            P(None, "tp"),
            P(None, "tp"),
            P("fs", "tp"),
            P("fs", "tp"),
            P("fs", "tp"),
            P("fs", "tp"),
        ),
        check_vma=False,
    )
```

profile of v0, /device:TPU:0, one launch (start us, length us, event | category | flops | bytes accessed | tf_op | source)
XLA Modules:
  0.0 73.2 jit_solution(17230720002343391033)
XLA Ops:
  0.6 70.7 %shard_map.186 = (f32[2,256,256]{2,1,0:T(8,128)S(1)}, f32[2,256,256]{2,1,0:T(8,128)S(1)}, bf16[2,8,256,256]{3,2,1,0:T(8,128)(2,1)S(1)}, f32[2,32,256]{2,1,0:T(8,128)S(1)}, f32[2,32,256]{2,1,0:T(8,128)S(1)}) custom-call(bf16[768,2048]{1,0:T(8,128)(2,1)} %saved_hbm.1, bf16[768,256]{1,0:T(8,128)(2,1)} %cot_in_hbm.1, bf16[768,256]{1,0:T(8,128)(2,1)} %cot_out_hbm.1, ...), custom_call_target="tpu_custom_call" | custom-call | tf_op jit(solution)/shard_map/pallas_call | solution.py:597
  71.4 1.8 %shard_map.187 = (f32[256,256]{1,0:T(8,128)}, f32[256,256]{1,0:T(8,128)}, f32[256,256]{1,0:T(8,128)}, f32[256,256]{1,0:T(8,128)}, bf16[2048,256]{1,0:T(8,128)(2,...) custom-call(f32[2,256,256]{2,1,0:T(8,128)S(1)} %get-tuple-element.15, ...), custom_call_target="tpu_custom_call" | custom-call | tf_op jit(solution)/shard_map/pallas_call | solution.py:633
where the time goes:
time: 73.3 us; the launch traced here: 73.2 us
  Pallas kernels  72.5 us (99%)
    pallas_call x1, Pallas kernels, kernel_form(): pl.pallas_call(functools.partial(kernel, n, tps, entries), out_shape=(sha...  70.7 us
    pallas_call x1, Pallas kernels, kernel_form(): pl.pallas_call(write_kernel, out_shape=(*[shape((rows, columns), F32)] *...  1.77 us

commit v1 on v0

--- a/solution.py
+++ b/solution.py
@@ -90,9 +90,7 @@
 
 def parts_of(x):
     high = x.astype(BF16)
-    rest = x - high.astype(F32)
-    middle = rest.astype(BF16)
-    return high, middle, (rest - middle.astype(F32)).astype(BF16)
+    return high, (x - high.astype(F32)).astype(BF16)
 
 
 def dot(a, b):
@@ -277,6 +275,157 @@
                     self.beside(c, neighbour).wait_send()
 
 
+class Late:
+    def __init__(self, place, chunks, ref_of, sems):
+        self.z, self.y, self.tp, self.depth = place
+        self.chunks, self.ref_of = chunks, ref_of
+        self.up_s, self.up_r, self.dn_s, self.dn_r, self.y_s, self.y_r, self.x_s, self.x_r = sems
+        self.last = self.depth - 1
+        self.at_end = (self.z == 0) | (self.z == self.last)
+        self.far = self.last - self.z
+        self.inner = jnp.where(self.z == 0, 1, self.last - 1)
+        self.outer = jnp.where(self.z == 1, 0, self.last)
+
+    def second(self, c):
+        return c >= self.chunks // 2
+
+    def copy(self, zi, yi, c, s_sem, r_sem, to_z, to_y):
+        ref = self.ref_of(zi * 2 + yi, c)
+        return pltpu.make_async_remote_copy(
+            src_ref=ref, dst_ref=ref, send_sem=s_sem, recv_sem=r_sem,
+            device_id=(to_z * 2 + to_y, self.tp), device_id_type=MESH,
+        )
+
+    def up(self, s, c):
+        return self.copy(self.z - s, self.y, c, self.up_s.at[s, c], self.up_r.at[s, c], self.z + 1, self.y)
+
+    def down(self, s, c):
+        return self.copy(self.z + s, self.y, c, self.dn_s.at[s, c], self.dn_r.at[s, c], self.z - 1, self.y)
+
+    def from_below(self, s, c):
+        return self.copy(self.z - 1 - s, self.y, c, self.up_s.at[s, c], self.up_r.at[s, c], self.z, self.y)
+
+    def from_above(self, s, c):
+        return self.copy(self.z + 1 + s, self.y, c, self.dn_s.at[s, c], self.dn_r.at[s, c], self.z, self.y)
+
+    def across(self, zi, c):
+        return self.copy(zi, self.y, c, self.y_s.at[zi, c], self.y_r.at[zi, c], self.z, 1 - self.y)
+
+    def from_across(self, zi, c):
+        return self.copy(zi, 1 - self.y, c, self.y_s.at[zi, c], self.y_r.at[zi, c], self.z, self.y)
+
+    def beside(self, zi, c, to_z):
+        return self.copy(zi, 1 - self.y, c, self.x_s.at[c], self.x_r.at[c], to_z, self.y)
+
+    def sidesteps(self, c):
+        return c >= 1
+
+    def crosses(self, zi, c):
+        gap = jnp.abs(self.z - zi)
+        near = jnp.where(self.at_end, True, zi != self.z)
+        if self.sidesteps(c):
+            near = near & jnp.logical_not(self.at_end & (gap == 1))
+        if self.second(c):
+            return near
+        near = near & jnp.logical_not(jnp.logical_not(self.at_end) & (gap == 2))
+        return near & (gap != self.last)
+
+    def goes_up(self, s):
+        return (self.z - s >= 0) & (self.z < self.last)
+
+    def goes_down(self, s):
+        return (self.z + s <= self.last) & (self.z >= 1)
+
+    def start_own(self, c):
+        @pl.when(self.goes_up(0))
+        def _():
+            self.up(0, c).start()
+
+        @pl.when(self.goes_down(0))
+        def _():
+            self.down(0, c).start()
+
+        @pl.when(self.at_end)
+        def _():
+            self.across(self.z, c).start()
+
+    def start_far(self, c):
+        if self.second(c):
+            self.across(self.far, c).start()
+        else:
+            self.beside(self.far, c, self.inner).start()
+
+    def start_beside(self, c):
+        if self.sidesteps(c):
+            self.beside(self.z, c, self.outer).start()
+
+    def hand_on(self, zi, c):
+        @pl.when(self.crosses(zi, c))
+        def _():
+            self.across(zi, c).start()
+
+    def relay(self):
+        z, depth = self.z, self.depth
+        for s in range(1, depth - 1):
+            for c in range(self.chunks):
+                @pl.when(z - s >= 0)
+                def _():
+                    self.from_below(s - 1, c).wait_recv()
+                    if s < depth - 2:
+                        @pl.when(z + 1 < depth)
+                        def _():
+                            self.up(s, c).start()
+                    self.hand_on(z - s, c)
+
+                @pl.when(z + s < depth)
+                def _():
+                    self.from_above(s - 1, c).wait_recv()
+                    if s < depth - 2:
+                        @pl.when(z >= 1)
+                        def _():
+                            self.down(s, c).start()
+                    self.hand_on(z + s, c)
+        for c in range(self.chunks):
+            for zi in range(depth):
+                @pl.when(self.crosses(zi, c))
+                def _():
+                    self.from_across(zi, c).wait_recv()
+            if not self.second(c):
+                @pl.when(jnp.logical_not(self.at_end))
+                def _():
+                    self.from_beside(self.last - self.outer, c).wait_recv()
+            if self.sidesteps(c):
+                @pl.when(self.at_end)
+                def _():
+                    self.from_beside(self.inner, c).wait_recv()
+
+    def from_beside(self, zi, c):
+        return self.copy(zi, 1 - self.y, c, self.x_s.at[c], self.x_r.at[c], self.z, self.y)
+
+    def finish(self):
+        for c in range(self.chunks):
+            for s in range(self.depth - 2):
+                @pl.when(self.goes_up(s))
+                def _():
+                    self.up(s, c).wait_send()
+
+                @pl.when(self.goes_down(s))
+                def _():
+                    self.down(s, c).wait_send()
+            for zi in range(self.depth):
+                @pl.when(self.crosses(zi, c))
+                def _():
+                    self.across(zi, c).wait_send()
+            if not self.second(c):
+                @pl.when(self.at_end)
+                def _():
+                    self.beside(self.far, c, self.inner).wait_send()
+            if self.sidesteps(c):
+                @pl.when(jnp.logical_not(self.at_end))
+                def _():
+                    self.beside(self.z, c, self.outer).wait_send()
+
+
 def gather_sems(depth, chunks):
     dma = pltpu.SemaphoreType.DMA
     return [dma((depth - 1, chunks))] * 4 + [dma((depth, chunks))] * 2 + [dma((chunks,))] * 2
@@ -365,37 +514,64 @@
             map_handed((z + distance) * 2 + 1 - y)
 
     at_end = (z == 0) | (z == depth - 1)
-    inner = jnp.where(z == 0, 1, depth - 2)
-    by_end = (z == 1) | (z == depth - 2)
-    outer = jnp.where(z == 1, 0, depth - 1)
+    middle = jnp.logical_not(at_end)
+    far = depth - 1 - z
 
     def early_cross(m, c):
-        return pltpu.make_async_remote_copy(
-            src_ref=weights.at[m, pl.ds(c * half, half)], dst_ref=early.at[0, m, pl.ds(c * half, half)],
+        part = pl.ds(c * half, half)
+        return pltpu.make_async_remote_copy(
+            src_ref=weights.at[m, part], dst_ref=early.at[0, m, part],
             send_sem=wy_s.at[m, c], recv_sem=wy_r.at[m, c], device_id=(z * 2 + 1 - y, tp), device_id_type=MESH,
         )
 
-    def early_along(m, c):
-        return pltpu.make_async_remote_copy(
-            src_ref=weights.at[m, pl.ds(c * half, half)], dst_ref=early.at[1, m, pl.ds(c * half, half)],
-            send_sem=wz_s.at[m, c], recv_sem=wz_r.at[m, c], device_id=(outer * 2 + y, tp), device_id_type=MESH,
-        )
-
-    def early_along_start(m):
-        @pl.when(by_end)
+    def early_far(m, c):
+        part = pl.ds(c * half, half)
+        return pltpu.make_async_remote_copy(
+            src_ref=weights.at[m, part], dst_ref=early.at[0, m, part],
+            send_sem=wz_s.at[m, c], recv_sem=wz_r.at[m, c], device_id=(far * 2 + y, tp), device_id_type=MESH,
+        )
+
+    def far_cross(c):
+        part = pl.ds(c * half, half)
+        return pltpu.make_async_remote_copy(
+            src_ref=early.at[0, 0, part], dst_ref=early.at[1, 0, part],
+            send_sem=wy_s.at[0, c], recv_sem=wy_r.at[0, c], device_id=(z * 2 + 1 - y, tp), device_id_type=MESH,
+        )
+
+    def far_start(m):
+        @pl.when(at_end)
         def _():
             for c in range(2):
-                early_along(m, c).start()
+                early_far(m, c).start()
+
+    def far_cross_start(c):
+        @pl.when(at_end)
+        def _():
+            early_far(0, c).wait_recv()
+            far_cross(c).start()
+
+    def cross_start(m, c):
+        @pl.when(middle)
+        def _():
+            early_cross(m, c).start()
+
+    def after_hop(s):
+        if s >= 2:
+            map_at(s - 2)
+        if s == 2:
+            loads[9].wait()
+            loads[10].wait()
+            far_start(0)
 
     map_block(me, True)
     gather.relay(
         lambda block, c: hand(side, block, c).start(),
-        lambda s: map_at(s - 2) if s >= 2 else None,
+        after_hop,
     )
-    for load in loads[3:]:
+    for load in loads[3:9]:
         load.wait()
-    early_cross(0, 0).start()
-    early_along_start(0)
+    cross_start(0, 0)
+    far_start(1)
     map_at(depth - 1)
 
     def term_cross(m, zi):
@@ -419,8 +595,8 @@
 
     order = [k % depth for k in range(1, depth + 1)]
     for m in range(2):
-        high, middle, low = parts_of(mapped[m].T)
-        term = dot(high, cots[m]) + (dot(middle, cots[m]) + dot(low, cots[m]))
+        high, rest = parts_of(mapped[m].T)
+        term = dot(high, cots[m]) + dot(rest, cots[m])
         terms[m] = term.reshape(n, slim, term.shape[1])
         for k in order:
             term_cross(m, (z + k) % depth).start()
@@ -432,7 +608,8 @@
             if k:
                 term_along(m, zi).start()
 
-    early_cross(0, 1).start()
+    cross_start(0, 1)
+    far_cross_start(0)
 
     def small_along(m, zi):
         ref = smalls.at[m, me]
@@ -487,24 +664,23 @@
             device_id=(me, tp), device_id_type=MESH,
         )
 
-    early_cross(1, 0).start()
-    early_cross(1, 1).start()
-    early_along_start(1)
+    cross_start(1, 0)
+    cross_start(1, 1)
+    far_cross_start(1)
 
     def chunk_ref(block, c):
         return copies.at[c // 2, block, pl.ds(c % 2 * half, half)]
 
-    copy_gather = Gather(place, 4, chunk_ref, gather_refs[8:], near=True)
+    late = Late(place, 4, chunk_ref, gather_refs[8:])
     beside = z * 2 + 1 - y
-    behind = inner * 2 + y
     for m in range(2):
         for k in range(depth):
             small_cross(m, (z + k) % depth, 1 - y).wait_recv()
-        high, middle, low = parts_of(smalls[m].reshape(n * slim, smalls.shape[3]))
+        high, rest = parts_of(smalls[m].reshape(n * slim, smalls.shape[3]))
 
         def full_of(block):
             factor = factors[m, block]
-            return dot(factor, high) + (dot(factor, middle) + dot(factor, low))
+            return dot(factor, high) + dot(factor, rest)
 
         total = None
         for block in range(n):
@@ -515,12 +691,13 @@
         for k in range(1, tps):
             send_square(m, k).start()
         update[m] = full_of(me)
-        ahead[0] = full_of(beside)
-
-        @pl.when(at_end)
-        def _():
-            ahead[1] = full_of(behind)
-
+        ahead[m, 0] = full_of(jnp.where(at_end, far * 2 + y, beside))
+        if m == 0:
+            @pl.when(at_end)
+            def _():
+                ahead[m, 1] = full_of(far * 2 + 1 - y)
+
+    for m in range(2):
         for k in range(1, tps):
             recv_square(m, k).wait_recv()
         mean = jnp.sum(jnp.sum(squares[m], axis=0), keepdims=True) / entries
@@ -529,32 +706,48 @@
         new_weight = weights[m] - 0.02 * new_update
         copies[m, me] = new_weight.astype(BF16)
         for c in range(2 * m, 2 * m + 2):
-            copy_gather.start(c)
+            late.start_own(c)
         update[m] = new_update
         fresh[m] = new_weight
+
+        @pl.when(middle)
+        def _():
+            for c in range(2):
+                early_cross(m, c).wait_recv()
+            copies[m, beside] = (early[0, m] - 0.02 * (ahead[m, 0] / root)).astype(BF16)
+            for c in range(2 * m, 2 * m + 2):
+                late.start_beside(c)
+
+        @pl.when(at_end)
+        def _():
+            for c in range(2):
+                if m == 0:
+                    far_cross(c).wait_recv()
+                else:
+                    early_far(m, c).wait_recv()
+            copies[m, far * 2 + y] = (early[0, m] - 0.02 * (ahead[m, 0] / root)).astype(BF16)
+            if m == 0:
+                copies[m, far * 2 + 1 - y] = (early[1, m] - 0.02 * (ahead[m, 1] / root)).astype(BF16)
+            for c in range(2 * m, 2 * m + 2):
+                late.start_far(c)
+
+    late.relay()
+
+    @pl.when(middle)
+    def _():
+        for m in range(2):
+            for c in range(2):
+                early_cross(m, c).wait_send()
+
+    @pl.when(at_end)
+    def _():
         for c in range(2):
-            early_cross(m, c).wait_recv()
-        copies[m, beside] = (early[0, m] - 0.02 * (ahead[0] / root)).astype(BF16)
-        for c in range(2 * m, 2 * m + 2):
-            copy_gather.start_beside(c)
-
-        @pl.when(at_end)
-        def _():
-            for c in range(2):
-                early_along(m, c).wait_recv()
-            copies[m, behind] = (early[1, m] - 0.02 * (ahead[1] / root)).astype(BF16)
-
-    copy_gather.relay()
-
-    for m in range(2):
-        for c in range(2):
-            early_cross(m, c).wait_send()
-
-            @pl.when(by_end)
-            def _():
-                early_along(m, c).wait_send()
+            far_cross(c).wait_send()
+            for m in range(2):
+                early_far(m, c).wait_send()
+
     gather.finish()
-    copy_gather.finish()
+    late.finish()
     for k in range(1, n):
         for c in range(2):
             hand(side, (me + k) % n, c).wait_send()
@@ -618,7 +811,7 @@
             pltpu.VMEM((2, n, slim, columns), F32),
             pltpu.VMEM((2, tps, 8, columns), F32),
             pltpu.VMEM((2, 2, rows, columns), F32),
-            pltpu.VMEM((2, rows, columns), F32),
+            pltpu.VMEM((2, 2, rows, columns), F32),
             *[dma((2, 2))] * 4,
             dma((11,)),
             dma((n, 2)), dma((n, 2)),
@@ -645,7 +838,7 @@
 def on_device(saved_input, cot_inproj, cot_outproj, factor_inproj, *others):
     n, tps = lax.axis_size("fs"), lax.axis_size("tp")
     rows, rank = factor_inproj.shape
-    if n % 2 == 0 and n >= 8 and tps % 2 == 0 and rank % (8 * n) == 0 and rows % 128 == 0 and cot_inproj.shape[1] % 128 == 0:
+    if n % 2 == 0 and n == 8 and tps % 2 == 0 and rank % (8 * n) == 0 and rows % 128 == 0 and cot_inproj.shape[1] % 128 == 0:
         return kernel_form(n, tps, saved_input, cot_inproj, cot_outproj, factor_inproj, *others)
     return plain_form(saved_input, cot_inproj, cot_outproj, factor_inproj, *others)
 

time: 73.3 us -> 73.6 us (level)
  no operation moved by 1% of the time
where the time goes in v1:
time: 73.6 us; the launch traced here: 73.4 us
  Pallas kernels  72.8 us (99%)
    pallas_call x1, Pallas kernels, kernel_form(): pl.pallas_call(functools.partial(kernel, n, tps, entries), out_shape=(sha...  71 us
    pallas_call x1, Pallas kernels, kernel_form(): pl.pallas_call(write_kernel, out_shape=(*[shape((rows, columns), F32)] *...  1.77 us

profile of v1, /device:TPU:0, one launch (start us, length us, event | category | flops | bytes accessed | tf_op | source)
XLA Modules:
  0.0 73.4 jit_solution(10093782909179036172)
XLA Ops:
  0.6 71.0 %shard_map.186 = (f32[2,256,256]{2,1,0:T(8,128)S(1)}, f32[2,256,256]{2,1,0:T(8,128)S(1)}, bf16[2,8,256,256]{3,2,1,0:T(8,128)(2,1)S(1)}, f32[2,32,256]{2,1,0:T(8,128)S(1)}, f32[2,32,256]{2,1,0:T(8,128)S(1)}) custom-call(bf16[768,2048]{1,0:T(8,128)(2,1)} %saved_hbm.1, bf16[768,256]{1,0:T(8,128)(2,1)} %cot_in_hbm.1, bf16[768,256]{1,0:T(8,128)(2,1)} %cot_out_hbm.1, ...), custom_call_target="tpu_custom_call" | custom-call | tf_op jit(solution)/shard_map/pallas_call | solution.py:790
  71.7 1.8 %shard_map.187 = (f32[256,256]{1,0:T(8,128)}, f32[256,256]{1,0:T(8,128)}, f32[256,256]{1,0:T(8,128)}, f32[256,256]{1,0:T(8,128)}, bf16[2048,256]{1,0:T(8,128)(2,...) custom-call(f32[2,256,256]{2,1,0:T(8,128)S(1)} %get-tuple-element.15, ...), custom_call_target="tpu_custom_call" | custom-call | tf_op jit(solution)/shard_map/pallas_call | solution.py:826

commit v2 on v0

v2 whole, which is shorter than its diff:
```python
import functools

import jax
import jax.numpy as jnp
from jax import lax
from jax.experimental import pallas as pl
from jax.experimental.pallas import tpu as pltpu
from jax.sharding import PartitionSpec as P


def contract_rows(left, right, precision):
    return lax.dot_general(
        left,
        right,
        (((0,), (0,)), ((), ())),
        precision=precision,
        preferred_element_type=jnp.float32,
    )


def plain_form(
    saved_input,
    cot_inproj,
    cot_outproj,
    factor_inproj,
    factor_outproj,
    weight_inproj,
    weight_outproj,
    first_inproj,
    first_outproj,
    second_inproj,
    second_outproj,
):
    highest = lax.Precision.HIGHEST
    pieces = (
        lax.all_gather(factor_inproj, "fs", axis=0, tiled=True),
        lax.all_gather(factor_outproj, "fs", axis=0, tiled=True),
    )
    mapped_in = jnp.dot(saved_input, pieces[0], preferred_element_type=jnp.float32)
    mapped_out = jnp.dot(saved_input, pieces[1], preferred_element_type=jnp.float32)
    term_in = contract_rows(mapped_in, cot_inproj.astype(jnp.float32), highest)
    term_out = contract_rows(mapped_out, cot_outproj.astype(jnp.float32), highest)
    projected_in, projected_out = (
        lax.psum_scatter(term_in, "fs", scatter_dimension=0, tiled=True),
        lax.psum_scatter(term_out, "fs", scatter_dimension=0, tiled=True),
    )
    first_in_new = 0.8 * first_inproj + 0.2 * projected_in
    first_out_new = 0.8 * first_outproj + 0.2 * projected_out
    second_in_new = 0.9 * second_inproj + 0.1 * projected_in * projected_in
    second_out_new = 0.9 * second_outproj + 0.1 * projected_out * projected_out
    small_in = first_in_new / (jnp.sqrt(second_in_new) + 1e-08)
    small_out = first_out_new / (jnp.sqrt(second_out_new) + 1e-08)
    wide_in = factor_inproj.astype(jnp.float32)
    wide_out = factor_outproj.astype(jnp.float32)
    pieces = (
        lax.all_gather(small_in, "fs", axis=0, tiled=True),
        lax.all_gather(small_out, "fs", axis=0, tiled=True),
    )
    full_in = jnp.dot(wide_in, pieces[0], precision=highest)
    full_out = jnp.dot(wide_out, pieces[1], precision=highest)
    square_in, square_out = lax.psum(
        (jnp.sum(full_in * full_in), jnp.sum(full_out * full_out)), ("fs", "tp")
    )
    entries = float(full_in.shape[0] * full_in.shape[1] * lax.axis_size("fs") * lax.axis_size("tp"))
    update_in = full_in / jnp.sqrt(square_in / entries + 1e-06)
    update_out = full_out / jnp.sqrt(square_out / entries + 1e-06)
    fresh_in = weight_inproj - 0.02 * update_in
    fresh_out = weight_outproj - 0.02 * update_out
    copy_in, copy_out = (
        lax.all_gather(fresh_in.astype(jnp.bfloat16), "fs", axis=0, tiled=True),
        lax.all_gather(fresh_out.astype(jnp.bfloat16), "fs", axis=0, tiled=True),
    )
    return (
        update_in,
        update_out,
        fresh_in,
        fresh_out,
        copy_in,
        copy_out,
        first_in_new,
        first_out_new,
        second_in_new,
        second_out_new,
    )


MESH = pl.DeviceIdType.MESH
F32, BF16 = jnp.float32, jnp.bfloat16


def parts_of(x):
    high = x.astype(BF16)
    return high, (x - high.astype(F32)).astype(BF16)


def dot(a, b):
    return jnp.dot(a, b, preferred_element_type=F32)


class Late:
    def __init__(self, place, chunks, ref_of, sems):
        self.z, self.y, self.tp, self.depth = place
        self.chunks, self.ref_of = chunks, ref_of
        self.up_s, self.up_r, self.dn_s, self.dn_r, self.y_s, self.y_r, self.x_s, self.x_r = sems
        self.last = self.depth - 1
        self.at_end = (self.z == 0) | (self.z == self.last)
        self.far = self.last - self.z
        self.inner = jnp.where(self.z == 0, 1, self.last - 1)
        self.outer = jnp.where(self.z == 1, 0, self.last)

    def second(self, c):
        return c >= self.chunks // 2

    def copy(self, zi, yi, c, s_sem, r_sem, to_z, to_y):
        ref = self.ref_of(zi * 2 + yi, c)
        return pltpu.make_async_remote_copy(
            src_ref=ref, dst_ref=ref, send_sem=s_sem, recv_sem=r_sem,
            device_id=(to_z * 2 + to_y, self.tp), device_id_type=MESH,
        )

    def up(self, s, c):
        return self.copy(self.z - s, self.y, c, self.up_s.at[s, c], self.up_r.at[s, c], self.z + 1, self.y)

    def down(self, s, c):
        return self.copy(self.z + s, self.y, c, self.dn_s.at[s, c], self.dn_r.at[s, c], self.z - 1, self.y)

    def from_below(self, s, c):
        return self.copy(self.z - 1 - s, self.y, c, self.up_s.at[s, c], self.up_r.at[s, c], self.z, self.y)

    def from_above(self, s, c):
        return self.copy(self.z + 1 + s, self.y, c, self.dn_s.at[s, c], self.dn_r.at[s, c], self.z, self.y)

    def across(self, zi, c):
        return self.copy(zi, self.y, c, self.y_s.at[zi, c], self.y_r.at[zi, c], self.z, 1 - self.y)

    def from_across(self, zi, c):
        return self.copy(zi, 1 - self.y, c, self.y_s.at[zi, c], self.y_r.at[zi, c], self.z, self.y)

    def beside(self, zi, c, to_z):
        return self.copy(zi, 1 - self.y, c, self.x_s.at[c], self.x_r.at[c], to_z, self.y)

    def crosses(self, zi, c):
        gap = jnp.abs(self.z - zi)
        near = gap < self.last
        if self.second(c):
            near = near & (gap != 1)
        return jnp.where(self.at_end, near, gap == 1)

    def goes_up(self, s):
        return (self.z - s >= 0) & (self.z < self.last)

    def goes_down(self, s):
        return (self.z + s <= self.last) & (self.z >= 1)

    def start_own(self, c):
        @pl.when(self.goes_up(0))
        def _():
            self.up(0, c).start()

        @pl.when(self.goes_down(0))
        def _():
            self.down(0, c).start()

        @pl.when(self.at_end)
        def _():
            self.across(self.z, c).start()

    def start_far(self, c):
        self.beside(self.far, c, self.inner).start()

    def start_beside(self, c):
        if self.second(c):
            self.beside(self.z, c, self.outer).start()

    def hand_on(self, zi, c):
        @pl.when(self.crosses(zi, c))
        def _():
            self.across(zi, c).start()

    def relay(self):
        z, depth = self.z, self.depth
        for s in range(1, depth - 1):
            for c in range(self.chunks):
                @pl.when(z - s >= 0)
                def _():
                    self.from_below(s - 1, c).wait_recv()
                    if s < depth - 2:
                        @pl.when(z + 1 < depth)
                        def _():
                            self.up(s, c).start()
                    self.hand_on(z - s, c)

                @pl.when(z + s < depth)
                def _():
                    self.from_above(s - 1, c).wait_recv()
                    if s < depth - 2:
                        @pl.when(z >= 1)
                        def _():
                            self.down(s, c).start()
                    self.hand_on(z + s, c)
        for c in range(self.chunks):
            for zi in range(depth):
                @pl.when(self.crosses(zi, c))
                def _():
                    self.from_across(zi, c).wait_recv()

            @pl.when(jnp.logical_not(self.at_end))
            def _():
                self.from_beside(self.last - self.outer, c).wait_recv()

            if self.second(c):
                @pl.when(self.at_end)
                def _():
                    self.from_beside(self.inner, c).wait_recv()

    def from_beside(self, zi, c):
        return self.copy(zi, 1 - self.y, c, self.x_s.at[c], self.x_r.at[c], self.z, self.y)

    def finish(self):
        for c in range(self.chunks):
            for s in range(self.depth - 2):
                @pl.when(self.goes_up(s))
                def _():
                    self.up(s, c).wait_send()

                @pl.when(self.goes_down(s))
                def _():
                    self.down(s, c).wait_send()
            for zi in range(self.depth):
                @pl.when(self.crosses(zi, c))
                def _():
                    self.across(zi, c).wait_send()

            @pl.when(self.at_end)
            def _():
                self.beside(self.far, c, self.inner).wait_send()

            if self.second(c):
                @pl.when(jnp.logical_not(self.at_end))
                def _():
                    self.beside(self.z, c, self.outer).wait_send()


def gather_sems(depth, chunks):
    dma = pltpu.SemaphoreType.DMA
    return [dma((depth - 1, chunks))] * 4 + [dma((depth, chunks))] * 2 + [dma((chunks,))] * 2


def kernel(
    n, tps, entries,
    saved_hbm, cot_in_hbm, cot_out_hbm, factor_in_hbm, factor_out_hbm, weight_in_hbm, weight_out_hbm,
    first_in_hbm, first_out_hbm, second_in_hbm, second_out_hbm,
    update, fresh, copies, first_new, second_new,
    saved, cots, cotx, factors, weights, first, second, moment, moment_new, mapped, terms, crossed, staged, landed,
    smalls, swapped, squares, early, ahead,
    load_sem, fz_s, fz_r, fy_s, fy_r, pair_s, pair_r, cot_s, cot_r, mom_s, mom_r, new_s, new_r, fx_s, fx_r, sx_s, sx_r,
    wy_s, wy_r, wz_s, wz_r, ty_s, ty_r, tz_s, tz_r, sz_s, sz_r, sy_s, sy_r, norm_s, norm_r, *gather_refs,
):
    me, tp = lax.axis_index("fs"), lax.axis_index("tp")
    z, y = me // 2, me % 2
    depth = n // 2
    last = depth - 1
    core, mine = tp % 2, tp // 2
    other = 1 - mine
    matrix = (mine, other)
    partner = mine * 2 + 1 - core
    opposite = other * 2 + core
    rows = factors.shape[2]
    half = rows // 2
    slim = first.shape[1]
    beside = z * 2 + 1 - y
    at_end = (z == 0) | (z == last)
    middle = jnp.logical_not(at_end)
    far = last - z

    barrier = pltpu.get_barrier_semaphore()
    for k in range(1, depth):
        pl.semaphore_signal(barrier, inc=1, device_id=((z + k) % depth * 2 + y, tp), device_id_type=MESH)
    pl.semaphore_signal(barrier, inc=1, device_id=(beside, tp), device_id_type=MESH)
    for k in range(1, tps):
        pl.semaphore_signal(barrier, inc=1, device_id=(me, (tp + k) % tps), device_id_type=MESH)

    loads = [
        pltpu.make_async_copy(source, target, load_sem.at[i])
        for i, (source, target) in enumerate((
            (factor_in_hbm, factors.at[0, me]), (factor_out_hbm, factors.at[1, me]),
            (cot_in_hbm, cots.at[0]), (cot_out_hbm, cots.at[1]),
            (saved_hbm, saved),
            (weight_in_hbm, weights.at[0]), (weight_out_hbm, weights.at[1]),
            (first_in_hbm, first.at[0]), (first_out_hbm, first.at[1]),
            (second_in_hbm, second.at[0]), (second_out_hbm, second.at[1]),
        ))
    ]
    for load in loads:
        load.start()
    loads[0].wait()
    loads[1].wait()
    pl.semaphore_wait(barrier, depth + tps - 1)

    def send(source, target, s_sem, r_sem, to_fs, to_tp):
        return pltpu.make_async_remote_copy(
            src_ref=source, dst_ref=target, send_sem=s_sem, recv_sem=r_sem,
            device_id=(to_fs, to_tp), device_id_type=MESH,
        )

    def factor_part(block):
        return factors.at[mine, block, pl.ds(core * half, half)]

    def factor_along(zi):
        ref = factor_part(me)
        return send(ref, ref, fz_s.at[zi], fz_r.at[z], zi * 2 + y, tp)

    def factor_from(zi):
        ref = factor_part(zi * 2 + y)
        return send(ref, ref, fz_s.at[zi], fz_r.at[zi], me, tp)

    def factor_cross(zi, column):
        ref = factor_part(zi * 2 + column)
        return send(ref, ref, fy_s.at[zi], fy_r.at[zi], beside, tp)

    def hand(block):
        ref = factor_part(block)
        return send(ref, ref, pair_s.at[block], pair_r.at[block], me, partner)

    def handed(block):
        ref = factors.at[mine, block, pl.ds((1 - core) * half, half)]
        return send(ref, ref, pair_s.at[block], pair_r.at[block], me, partner)

    near_one = jnp.where(z % 2 == 0, 1, last - 1)
    far_one = jnp.where(z < depth // 2, last, 0)
    third = jnp.where(z == 0, last - 1, jnp.where(z == last, 1, jnp.where(z == 1, 0, last)))
    factor_along(jnp.where(at_end, far_one, near_one)).start()
    factor_cross(z, y).start()
    factor_along(jnp.where(at_end, third, far_one)).start()
    factor_along(jnp.where(at_end, near_one, third)).start()

    loads[2].wait()
    loads[3].wait()
    cot_swap = send(cots.at[other], cotx, cot_s, cot_r, me, opposite)
    cot_swap.start()

    part_of = lambda c: pl.ds(c * half, half)

    def early_cross(o, c):
        return send(weights.at[matrix[o], part_of(c)], early.at[0, o, part_of(c)], wy_s.at[o, c], wy_r.at[o, c], beside, tp)

    def early_far(o, c):
        return send(
            weights.at[matrix[o], part_of(c)], early.at[0, o, part_of(c)], wz_s.at[o, c], wz_r.at[o, c], far * 2 + y, tp
        )

    def far_cross(o, c):
        return send(early.at[0, o, part_of(c)], early.at[1, o, part_of(c)], wy_s.at[o, c], wy_r.at[o, c], beside, tp)

    def early_start(o, c):
        @pl.when(middle)
        def _():
            early_cross(o, c).start()

    def far_start(o, c):
        @pl.when(at_end)
        def _():
            early_far(o, c).wait_recv()
            far_cross(o, c).start()

    loads[5].wait()
    loads[6].wait()

    @pl.when(at_end)
    def _():
        for o in range(2):
            for c in range(2):
                early_far(o, c).start()

    loads[4].wait()

    def map_block(block, first_one=False):
        piece = saved[:, pl.ds(pl.multiple_of(block * rows, rows), rows)]
        product = dot(piece, factors[mine, block])
        mapped[...] = product if first_one else mapped[...] + product

    def map_handed(block):
        handed(block).wait_recv()
        map_block(block)

    def take_along(zi):
        factor_from(zi).wait_recv()
        factor_cross(zi, y).start()
        hand(zi * 2 + y).start()

    def take_cross(zi):
        factor_cross(zi, 1 - y).wait_recv()
        hand(zi * 2 + 1 - y).start()

    map_block(me, True)
    take_along(near_one)
    take_cross(z)
    take_along(far_one)
    map_handed(near_one * 2 + y)
    map_handed(beside)
    take_along(third)
    take_cross(near_one)
    early_start(0, 0)
    early_start(0, 1)
    map_handed(far_one * 2 + y)
    map_handed(near_one * 2 + 1 - y)
    take_cross(far_one)
    map_handed(third * 2 + y)
    map_handed(far_one * 2 + 1 - y)
    take_cross(third)
    for load in loads[7:]:
        load.wait()
    moment_swap = [
        send(source.at[other], moment.at[i], mom_s.at[i], mom_r.at[i], me, opposite) for i, source in enumerate((first, second))
    ]
    for copy in moment_swap:
        copy.start()
    needed = (jnp.where(at_end, far * 2 + y, beside), jnp.where(at_end, far * 2 + 1 - y, beside))

    def factor_swap(i, m):
        ref = factors.at[m, needed[i]]
        return send(ref, ref, fx_s.at[i], fx_r.at[i], me, opposite)

    map_handed(third * 2 + 1 - y)

    def term_cross(s, zi):
        return send(terms.at[s, zi * 2 + 1 - y], crossed.at[s, zi], ty_s.at[s, zi], ty_r.at[s, zi], beside, tp)

    def term_along(s, zi):
        return send(staged.at[s, zi], landed.at[s, z], tz_s.at[s, zi], tz_r.at[s, z], zi * 2 + y, tp)

    def term_from(s, zi):
        return send(staged.at[s, z], landed.at[s, zi], tz_s.at[s, z], tz_r.at[s, zi], me, tp)

    order = [k % depth for k in range(1, depth + 1)]
    high, rest = parts_of(mapped[...].T)
    for s in range(2):
        if s == 0:
            cot = cots[mine]
        else:
            cot_swap.wait_recv()
            cot = cotx[...]
        term = dot(high, cot) + dot(rest, cot)
        terms[s] = term.reshape(n, slim, term.shape[1])
        for k in order:
            term_cross(s, (z + k) % depth).start()
    factor_swap(0, mine).start()

    @pl.when(at_end)
    def _():
        factor_swap(1, mine).start()

    for s in range(2):
        for k in order:
            zi = (z + k) % depth
            term_cross(s, zi).wait_recv()
            staged[s, zi] = terms[s, zi * 2 + y] + crossed[s, zi]
            if k:
                term_along(s, zi).start()
    early_start(1, 0)
    far_start(0, 0)
    far_start(0, 1)

    def small_along(s, zi):
        ref = smalls.at[s, me]
        return send(ref, ref, sz_s.at[s, zi], sz_r.at[s, z], zi * 2 + y, tp)

    def small_from(s, zi):
        ref = smalls.at[s, zi * 2 + y]
        return send(ref, ref, sz_s.at[s, zi], sz_r.at[s, zi], me, tp)

    def small_cross(s, zi, column):
        ref = smalls.at[s, zi * 2 + column]
        return send(ref, ref, sy_s.at[s, zi], sy_r.at[s, zi], beside, tp)

    def small_swap(block):
        return send(smalls.at[1, block], swapped.at[block], sx_s.at[block], sx_r.at[block], me, opposite)

    def new_swap(i):
        return send(moment_new.at[i], (first_new, second_new)[i].at[mine], new_s.at[i], new_r.at[i], me, opposite)

    for s in range(2):
        here = staged[s, z]
        for k in range(1, depth):
            term_from(s, (z + k) % depth).wait_recv()
            here = here + landed[s, (z + k) % depth]
        if s == 0:
            old_first, old_second = first[mine], second[mine]
        else:
            for copy in moment_swap:
                copy.wait_recv()
            old_first, old_second = moment[0], moment[1]
        new_first = 0.8 * old_first + 0.2 * here
        new_second = 0.9 * old_second + 0.1 * here * here
        smalls[s, me] = new_first / (jnp.sqrt(new_second) + 1e-08)
        for k in range(1, depth):
            small_along(s, (z + k) % depth).start()
        small_cross(s, z, y).start()
        if s == 0:
            first_new[mine] = new_first
            second_new[mine] = new_second
        else:
            small_swap(me).start()
            moment_new[0] = new_first
            moment_new[1] = new_second
    for s in range(2):
        for k in range(1, depth):
            zi = (z + k) % depth
            small_from(s, zi).wait_recv()
            small_cross(s, zi, y).start()
            if s == 1:
                small_swap(zi * 2 + y).start()
    early_start(1, 1)
    far_start(1, 0)
    far_start(1, 1)

    def send_square(k):
        return send(squares.at[tp], squares.at[tp], norm_s.at[k], norm_r.at[k], me, (tp + k) % tps)

    def recv_square(k):
        ref = squares.at[(tp + tps - k) % tps]
        return send(ref, ref, norm_s.at[k], norm_r.at[k], me, tp)

    def full_of(m, block, pieces):
        factor = factors[m, block]
        return dot(factor, pieces[0]) + dot(factor, pieces[1])

    columns = smalls.shape[3]
    total = None
    for s in range(2):
        for k in range(depth):
            zi = (z + k) % depth
            small_cross(s, zi, 1 - y).wait_recv()
            if s == 1:
                small_swap(zi * 2 + 1 - y).start()
        pieces = parts_of(smalls[s].reshape(n * slim, columns))
        for block in range(n):
            full = full_of(mine, block, pieces)
            square = jnp.sum((full * full).reshape(rows // 8, 8, columns), axis=0)
            total = square if total is None else total + square
        if s == 0:
            own_pieces = pieces
    squares[tp] = total
    for k in range(1, tps):
        send_square(k).start()
    for i in range(2):
        new_swap(i).start()

    def chunk_ref(block, c):
        return copies.at[matrix[c // 2], block, pl.ds(c % 2 * half, half)]

    late = Late((z, y, tp, depth), 4, chunk_ref, gather_refs)

    def fill_full(m, pieces):
        update[m] = full_of(m, me, pieces)
        ahead[0] = full_of(m, needed[0], pieces)

        @pl.when(at_end)
        def _():
            ahead[1] = full_of(m, needed[1], pieces)

    def root_of(m):
        mean = jnp.sum(squares[2 * m] + squares[2 * m + 1], keepdims=True) / entries
        return jnp.sqrt(mean + 1e-06)

    for o in range(2):
        m = matrix[o]
        if o == 0:
            fill_full(m, own_pieces)
            for k in range(1, tps):
                recv_square(k).wait_recv()
        else:
            for block in range(n):
                small_swap(block).wait_recv()
            factor_swap(0, other).wait_recv()

            @pl.when(at_end)
            def _():
                factor_swap(1, other).wait_recv()

            fill_full(m, parts_of(swapped[...].reshape(n * slim, columns)))
        root = root_of(m)
        new_update = update[m] / root
        new_weight = weights[m] - 0.02 * new_update
        copies[m, me] = new_weight.astype(BF16)
        for c in range(2 * o, 2 * o + 2):
            late.start_own(c)
        update[m] = new_update
        fresh[m] = new_weight

        @pl.when(middle)
        def _():
            for c in range(2):
                early_cross(o, c).wait_recv()
            copies[m, beside] = (early[0, o] - 0.02 * (ahead[0] / root)).astype(BF16)
            for c in range(2 * o, 2 * o + 2):
                late.start_beside(c)

        @pl.when(at_end)
        def _():
            for c in range(2):
                far_cross(o, c).wait_recv()
            copies[m, far * 2 + 1 - y] = (early[1, o] - 0.02 * (ahead[1] / root)).astype(BF16)
            for c in range(2 * o, 2 * o + 2):
                late.start_far(c)
            copies[m, far * 2 + y] = (early[0, o] - 0.02 * (ahead[0] / root)).astype(BF16)

    late.relay()
    for i in range(2):
        new_swap(i).wait_recv()

    @pl.when(middle)
    def _():
        for o in range(2):
            for c in range(2):
                early_cross(o, c).wait_send()

    @pl.when(at_end)
    def _():
        for o in range(2):
            for c in range(2):
                far_cross(o, c).wait_send()
                early_far(o, c).wait_send()
        factor_swap(1, mine).wait_send()

    factor_swap(0, mine).wait_send()
    late.finish()
    cot_swap.wait_send()
    for i in range(2):
        moment_swap[i].wait_send()
        new_swap(i).wait_send()
    for k in range(1, n):
        hand((me + k) % n).wait_send()
    for k in range(n):
        small_swap(k).wait_send()
    for k in range(depth):
        zi = (z + k) % depth
        factor_cross(zi, y).wait_send()
        if k:
            factor_along(zi).wait_send()
        for s in range(2):
            term_cross(s, zi).wait_send()
            small_cross(s, zi, y).wait_send()
            if k:
                term_along(s, zi).wait_send()
                small_along(s, zi).wait_send()
    for k in range(1, tps):
        send_square(k).wait_send()


def write_kernel(update, fresh, copies, first_new, second_new, *refs):
    outs, sem = refs[:-1], refs[-1]
    started = []
    for i, source in enumerate((update, fresh, copies, first_new, second_new)):
        for m in range(2):
            copy = pltpu.make_async_copy(source.at[m], outs[2 * i + m], sem.at[2 * i + m])
            copy.start()
            started.append(copy)
    for copy in started:
        copy.wait()


def kernel_form(n, tps, saved_input, cot_inproj, cot_outproj, factor_inproj, *others):
    tokens, wide = saved_input.shape
    columns = cot_inproj.shape[1]
    rows, rank = factor_inproj.shape
    slim = rank // n
    depth = n // 2
    entries = float(wide * columns * tps)
    dma = pltpu.SemaphoreType.DMA
    vmem = pl.BlockSpec(memory_space=pltpu.VMEM)
    anywhere = pl.BlockSpec(memory_space=pl.ANY)
    far = pl.BlockSpec(memory_space=pltpu.HBM)
    shape = jax.ShapeDtypeStruct
    results = pl.pallas_call(
        functools.partial(kernel, n, tps, entries),
        out_shape=(
            shape((2, rows, columns), F32), shape((2, rows, columns), F32),
            shape((2, n, rows, columns), BF16),
            shape((2, slim, columns), F32), shape((2, slim, columns), F32),
        ),
        in_specs=[far] * 11,
        out_specs=[vmem] * 5,
        scratch_shapes=[
            pltpu.VMEM((tokens, wide), BF16),
            pltpu.VMEM((2, tokens, columns), BF16),
            pltpu.VMEM((tokens, columns), BF16),
            pltpu.VMEM((2, n, rows, rank), BF16),
            pltpu.VMEM((2, rows, columns), F32),
            *[pltpu.VMEM((2, slim, columns), F32)] * 4,
            pltpu.VMEM((tokens, rank), F32),
            pltpu.VMEM((2, n, slim, columns), F32),
            *[pltpu.VMEM((2, depth, slim, columns), F32)] * 3,
            pltpu.VMEM((2, n, slim, columns), F32),
            pltpu.VMEM((n, slim, columns), F32),
            pltpu.VMEM((tps, 8, columns), F32),
            pltpu.VMEM((2, 2, rows, columns), F32),
            pltpu.VMEM((2, rows, columns), F32),
            dma((11,)),
            *[dma((depth,))] * 4,
            dma((n,)), dma((n,)),
            dma, dma,
            *[dma((2,))] * 6,
            dma((n,)), dma((n,)),
            *[dma((2, 2))] * 4,
            *[dma((2, depth))] * 8,
            dma((tps,)), dma((tps,)),
            *gather_sems(depth, 4),
        ],
        compiler_params=pltpu.CompilerParams(collective_id=0, has_side_effects=True, vmem_limit_bytes=40 * 2**20),
    )(*[pltpu.with_memory_space_constraint(x, pltpu.HBM) for x in (saved_input, cot_inproj, cot_outproj, factor_inproj, *others)])
    update, fresh, copies, first_new, second_new = results
    copies = copies.reshape(2, n * rows, columns)
    return pl.pallas_call(
        write_kernel,
        out_shape=(
            *[shape((rows, columns), F32)] * 4, *[shape((n * rows, columns), BF16)] * 2, *[shape((slim, columns), F32)] * 4,
        ),
        in_specs=[anywhere] * 5,
        out_specs=[far] * 10,
        scratch_shapes=[dma((10,))],
        compiler_params=pltpu.CompilerParams(vmem_limit_bytes=2**20),
    )(update, fresh, copies, first_new, second_new)


def on_device(saved_input, cot_inproj, cot_outproj, factor_inproj, *others):
    n, tps = lax.axis_size("fs"), lax.axis_size("tp")
    rows, rank = factor_inproj.shape
    if n == 8 and tps == 4 and rank % (8 * n) == 0 and rows % 128 == 0 and cot_inproj.shape[1] % 128 == 0:
        return kernel_form(n, tps, saved_input, cot_inproj, cot_outproj, factor_inproj, *others)
    return plain_form(saved_input, cot_inproj, cot_outproj, factor_inproj, *others)


def solution(mesh):
    return jax.shard_map(
        on_device,
        mesh=mesh,
        in_specs=(
            P("fs", None),
            P("fs", "tp"),
            P("fs", "tp"),
            P("fs", None),
            P("fs", None),
            P("fs", "tp"),
            P("fs", "tp"),
            P("fs", "tp"),
            P("fs", "tp"),
            P("fs", "tp"),
            P("fs", "tp"),
        ),
        out_specs=(
            P("fs", "tp"),
            P("fs", "tp"),
            P("fs", "tp"),
            P("fs", "tp"),
            P(None, "tp"),
            P(None, "tp"),
            P("fs", "tp"),
            P("fs", "tp"),
            P("fs", "tp"),
            P("fs", "tp"),
        ),
        check_vma=False,
    )
```

time: 73.3 us -> 76.5 us (1.044)
  Pallas kernels: 72.5 us -> 75.7 us
    pallas_call x1, Pallas kernels: 70.7 us -> 73.9 us  [kernel_form(): pl.pallas_call(functools.partial(kernel, n, tps, entries), out_shape=(sha...]
where the time goes in v2:
time: 76.5 us; the launch traced here: 76.3 us
  Pallas kernels  75.7 us (99%)
    pallas_call x1, Pallas kernels, kernel_form(): pl.pallas_call(functools.partial(kernel, n, tps, entries), out_shape=(sha...  73.9 us
    pallas_call x1, Pallas kernels, kernel_form(): pl.pallas_call(write_kernel, out_shape=(*[shape((rows, columns), F32)] *...  1.77 us

profile of v2, /device:TPU:0, one launch (start us, length us, event | category | flops | bytes accessed | tf_op | source)
XLA Modules:
  0.0 76.3 jit_solution(8765019007506309413)
XLA Ops:
  0.6 73.9 %shard_map.186 = (f32[2,256,256]{2,1,0:T(8,128)S(1)}, f32[2,256,256]{2,1,0:T(8,128)S(1)}, bf16[2,8,256,256]{3,2,1,0:T(8,128)(2,1)S(1)}, f32[2,32,256]{2,1,0:T(8,128)S(1)}, f32[2,32,256]{2,1,0:T(8,128)S(1)}) custom-call(bf16[768,2048]{1,0:T(8,128)(2,1)} %saved_hbm.1, bf16[768,256]{1,0:T(8,128)(2,1)} %cot_in_hbm.1, bf16[768,256]{1,0:T(8,128)(2,1)} %cot_out_hbm.1, ...), custom_call_target="tpu_custom_call" | custom-call | tf_op jit(solution)/shard_map/pallas_call | solution.py:675
  74.6 1.8 %shard_map.187 = (f32[256,256]{1,0:T(8,128)}, f32[256,256]{1,0:T(8,128)}, f32[256,256]{1,0:T(8,128)}, f32[256,256]{1,0:T(8,128)}, bf16[2048,256]{1,0:T(8,128)(2,...) custom-call(f32[2,256,256]{2,1,0:T(8,128)S(1)} %get-tuple-element.15, ...), custom_call_target="tpu_custom_call" | custom-call | tf_op jit(solution)/shard_map/pallas_call | solution.py:714

commit v3 on v2

--- a/solution.py
+++ b/solution.py
@@ -108,9 +108,6 @@
         self.inner = jnp.where(self.z == 0, 1, self.last - 1)
         self.outer = jnp.where(self.z == 1, 0, self.last)
 
-    def second(self, c):
-        return c >= self.chunks // 2
-
     def copy(self, zi, yi, c, s_sem, r_sem, to_z, to_y):
         ref = self.ref_of(zi * 2 + yi, c)
         return pltpu.make_async_remote_copy(
@@ -139,11 +136,19 @@
     def beside(self, zi, c, to_z):
         return self.copy(zi, 1 - self.y, c, self.x_s.at[c], self.x_r.at[c], to_z, self.y)
 
+    def sidesteps(self, c):
+        return 1 <= c and not self.plain(c)
+
+    def plain(self, c):
+        return c == self.chunks - 1
+
     def crosses(self, zi, c):
         gap = jnp.abs(self.z - zi)
         near = gap < self.last
-        if self.second(c):
+        if self.sidesteps(c):
             near = near & (gap != 1)
+        if self.plain(c):
+            return (gap >= 0)
         return jnp.where(self.at_end, near, gap == 1)
 
     def goes_up(self, s):
@@ -161,15 +166,18 @@
         def _():
             self.down(0, c).start()
 
-        @pl.when(self.at_end)
+        @pl.when(self.crosses(self.z, c))
         def _():
             self.across(self.z, c).start()
 
     def start_far(self, c):
-        self.beside(self.far, c, self.inner).start()
+        if self.plain(c):
+            self.across(self.far, c).start()
+        else:
+            self.beside(self.far, c, self.inner).start()
 
     def start_beside(self, c):
-        if self.second(c):
+        if self.sidesteps(c):
             self.beside(self.z, c, self.outer).start()
 
     def hand_on(self, zi, c):
@@ -203,12 +211,11 @@
                 @pl.when(self.crosses(zi, c))
                 def _():
                     self.from_across(zi, c).wait_recv()
-
-            @pl.when(jnp.logical_not(self.at_end))
-            def _():
-                self.from_beside(self.last - self.outer, c).wait_recv()
-
-            if self.second(c):
+            if not self.plain(c):
+                @pl.when(jnp.logical_not(self.at_end))
+                def _():
+                    self.from_beside(self.last - self.outer, c).wait_recv()
+            if self.sidesteps(c):
                 @pl.when(self.at_end)
                 def _():
                     self.from_beside(self.inner, c).wait_recv()
@@ -230,12 +237,11 @@
                 @pl.when(self.crosses(zi, c))
                 def _():
                     self.across(zi, c).wait_send()
-
-            @pl.when(self.at_end)
-            def _():
-                self.beside(self.far, c, self.inner).wait_send()
-
-            if self.second(c):
+            if not self.plain(c):
+                @pl.when(self.at_end)
+                def _():
+                    self.beside(self.far, c, self.inner).wait_send()
+            if self.sidesteps(c):
                 @pl.when(jnp.logical_not(self.at_end))
                 def _():
                     self.beside(self.z, c, self.outer).wait_send()
@@ -329,10 +335,10 @@
     near_one = jnp.where(z % 2 == 0, 1, last - 1)
     far_one = jnp.where(z < depth // 2, last, 0)
     third = jnp.where(z == 0, last - 1, jnp.where(z == last, 1, jnp.where(z == 1, 0, last)))
-    factor_along(jnp.where(at_end, far_one, near_one)).start()
+    factor_along(near_one).start()
     factor_cross(z, y).start()
-    factor_along(jnp.where(at_end, third, far_one)).start()
-    factor_along(jnp.where(at_end, near_one, third)).start()
+    factor_along(third).start()
+    factor_along(far_one).start()
 
     loads[2].wait()
     loads[3].wait()
@@ -363,6 +369,32 @@
             early_far(o, c).wait_recv()
             far_cross(o, c).start()
 
+    loads[4].wait()
+
+    def map_block(block, first_one=False):
+        piece = saved[:, pl.ds(pl.multiple_of(block * rows, rows), rows)]
+        product = dot(piece, factors[mine, block])
+        mapped[...] = product if first_one else mapped[...] + product
+
+    def map_handed(block):
+        handed(block).wait_recv()
+        map_block(block)
+
+    def take_along(zi):
+        factor_from(zi).wait_recv()
+        factor_cross(zi, y).start()
+        hand(zi * 2 + y).start()
+
+    def take_cross(zi):
+        factor_cross(zi, 1 - y).wait_recv()
+        hand(zi * 2 + 1 - y).start()
+
+    map_block(me, True)
+    take_along(near_one)
+    take_along(third)
+    take_cross(z)
+    map_handed(near_one * 2 + y)
+    take_along(far_one)
     loads[5].wait()
     loads[6].wait()
 
@@ -372,42 +404,14 @@
             for c in range(2):
                 early_far(o, c).start()
 
-    loads[4].wait()
-
-    def map_block(block, first_one=False):
-        piece = saved[:, pl.ds(pl.multiple_of(block * rows, rows), rows)]
-        product = dot(piece, factors[mine, block])
-        mapped[...] = product if first_one else mapped[...] + product
-
-    def map_handed(block):
-        handed(block).wait_recv()
-        map_block(block)
-
-    def take_along(zi):
-        factor_from(zi).wait_recv()
-        factor_cross(zi, y).start()
-        hand(zi * 2 + y).start()
-
-    def take_cross(zi):
-        factor_cross(zi, 1 - y).wait_recv()
-        hand(zi * 2 + 1 - y).start()
-
-    map_block(me, True)
-    take_along(near_one)
-    take_cross(z)
-    take_along(far_one)
-    map_handed(near_one * 2 + y)
+    map_handed(third * 2 + y)
     map_handed(beside)
-    take_along(third)
     take_cross(near_one)
-    early_start(0, 0)
-    early_start(0, 1)
+    take_cross(third)
+    map_handed(near_one * 2 + 1 - y)
     map_handed(far_one * 2 + y)
-    map_handed(near_one * 2 + 1 - y)
     take_cross(far_one)
-    map_handed(third * 2 + y)
-    map_handed(far_one * 2 + 1 - y)
-    take_cross(third)
+    map_handed(third * 2 + 1 - y)
     for load in loads[7:]:
         load.wait()
     moment_swap = [
@@ -421,7 +425,7 @@
         ref = factors.at[m, needed[i]]
         return send(ref, ref, fx_s.at[i], fx_r.at[i], me, opposite)
 
-    map_handed(third * 2 + 1 - y)
+    map_handed(far_one * 2 + 1 - y)
 
     def term_cross(s, zi):
         return send(terms.at[s, zi * 2 + 1 - y], crossed.at[s, zi], ty_s.at[s, zi], ty_r.at[s, zi], beside, tp)
@@ -457,9 +461,8 @@
             staged[s, zi] = terms[s, zi * 2 + y] + crossed[s, zi]
             if k:
                 term_along(s, zi).start()
-    early_start(1, 0)
+    early_start(0, 0)
     far_start(0, 0)
-    far_start(0, 1)
 
     def small_along(s, zi):
         ref = smalls.at[s, me]
@@ -510,9 +513,9 @@
             small_cross(s, zi, y).start()
             if s == 1:
                 small_swap(zi * 2 + y).start()
-    early_start(1, 1)
-    far_start(1, 0)
-    far_start(1, 1)
+    for o, c in ((0, 1), (1, 0)):
+        early_start(o, c)
+        far_start(o, c)
 
     def send_square(k):
         return send(squares.at[tp], squares.at[tp], norm_s.at[k], norm_r.at[k], me, (tp + k) % tps)
@@ -567,9 +570,10 @@
         m = matrix[o]
         if o == 0:
             fill_full(m, own_pieces)
-            for k in range(1, tps):
-                recv_square(k).wait_recv()
+            recv_square((tp + tps - partner) % tps).wait_recv()
         else:
+            for k in range(2):
+                recv_square((tp + tps - other * 2 - k) % tps).wait_recv()
             for block in range(n):
                 small_swap(block).wait_recv()
             factor_swap(0, other).wait_recv()
@@ -588,22 +592,30 @@
         update[m] = new_update
         fresh[m] = new_weight
 
+        def fill(block, c, slot):
+            copies[m, block, part_of(c)] = (early[slot, o, part_of(c)] - 0.02 * (ahead[slot, part_of(c)] / root)).astype(BF16)
+
+        halves = [c for c in range(2) if not late.plain(2 * o + c)]
+
         @pl.when(middle)
         def _():
+            for c in halves:
+                early_cross(o, c).wait_recv()
+                fill(beside, c, 0)
+                late.start_beside(2 * o + c)
+
+        @pl.when(at_end)
+        def _():
             for c in range(2):
-                early_cross(o, c).wait_recv()
-            copies[m, beside] = (early[0, o] - 0.02 * (ahead[0] / root)).astype(BF16)
-            for c in range(2 * o, 2 * o + 2):
-                late.start_beside(c)
-
-        @pl.when(at_end)
-        def _():
-            for c in range(2):
-                far_cross(o, c).wait_recv()
-            copies[m, far * 2 + 1 - y] = (early[1, o] - 0.02 * (ahead[1] / root)).astype(BF16)
-            for c in range(2 * o, 2 * o + 2):
-                late.start_far(c)
-            copies[m, far * 2 + y] = (early[0, o] - 0.02 * (ahead[0] / root)).astype(BF16)
+                if c in halves:
+                    far_cross(o, c).wait_recv()
+                    fill(far * 2 + 1 - y, c, 1)
+                else:
+                    early_far(o, c).wait_recv()
+                    fill(far * 2 + y, c, 0)
+                late.start_far(2 * o + c)
+            for c in halves:
+                fill(far * 2 + y, c, 0)
 
     late.relay()
     for i in range(2):
@@ -611,16 +623,15 @@
 
     @pl.when(middle)
     def _():
-        for o in range(2):
-            for c in range(2):
-                early_cross(o, c).wait_send()
+        for o, c in ((0, 0), (0, 1), (1, 0)):
+            early_cross(o, c).wait_send()
 
     @pl.when(at_end)
     def _():
-        for o in range(2):
-            for c in range(2):
+        for o, c in ((0, 0), (0, 1), (1, 0), (1, 1)):
+            if not late.plain(2 * o + c):
                 far_cross(o, c).wait_send()
-                early_far(o, c).wait_send()
+            early_far(o, c).wait_send()
         factor_swap(1, mine).wait_send()
 
     factor_swap(0, mine).wait_send()

time: 76.5 us -> 66.9 us (0.87)
  Pallas kernels: 75.7 us -> 66.1 us
    pallas_call x1, Pallas kernels: 73.9 us -> 64.4 us  [kernel_form(): pl.pallas_call(functools.partial(kernel, n, tps, entries), out_shape=(sha...]
where the time goes in v3:
time: 66.9 us; the launch traced here: 66.8 us
  Pallas kernels  66.1 us (99%)
    pallas_call x1, Pallas kernels, kernel_form(): pl.pallas_call(functools.partial(kernel, n, tps, entries), out_shape=(sha...  64.4 us
    pallas_call x1, Pallas kernels, kernel_form(): pl.pallas_call(write_kernel, out_shape=(*[shape((rows, columns), F32)] *...  1.77 us

profile of v3, /device:TPU:0, one launch (start us, length us, event | category | flops | bytes accessed | tf_op | source)
XLA Modules:
  0.0 66.8 jit_solution(8779889056486961153)
XLA Ops:
  0.6 64.4 %shard_map.186 = (f32[2,256,256]{2,1,0:T(8,128)S(1)}, f32[2,256,256]{2,1,0:T(8,128)S(1)}, bf16[2,8,256,256]{3,2,1,0:T(8,128)(2,1)S(1)}, f32[2,32,256]{2,1,0:T(8,128)S(1)}, f32[2,32,256]{2,1,0:T(8,128)S(1)}) custom-call(bf16[768,2048]{1,0:T(8,128)(2,1)} %saved_hbm.1, bf16[768,256]{1,0:T(8,128)(2,1)} %cot_in_hbm.1, bf16[768,256]{1,0:T(8,128)(2,1)} %cot_out_hbm.1, ...), custom_call_target="tpu_custom_call" | custom-call | tf_op jit(solution)/shard_map/pallas_call | solution.py:686
  65.0 1.8 %shard_map.187 = (f32[256,256]{1,0:T(8,128)}, f32[256,256]{1,0:T(8,128)}, f32[256,256]{1,0:T(8,128)}, f32[256,256]{1,0:T(8,128)}, bf16[2048,256]{1,0:T(8,128)(2,...) custom-call(f32[2,256,256]{2,1,0:T(8,128)S(1)} %get-tuple-element.15, ...), custom_call_target="tpu_custom_call" | custom-call | tf_op jit(solution)/shard_map/pallas_call | solution.py:725

commit v4 on v3

--- a/solution.py
+++ b/solution.py
@@ -97,6 +97,9 @@
     return jnp.dot(a, b, preferred_element_type=F32)
 
 
+END_OWN, MID_OWN, END_FAR = (2, 3), (2, 3), (0, 1)
+
+
 class Late:
     def __init__(self, place, chunks, ref_of, sems):
         self.z, self.y, self.tp, self.depth = place
@@ -133,23 +136,29 @@
     def from_across(self, zi, c):
         return self.copy(zi, 1 - self.y, c, self.y_s.at[zi, c], self.y_r.at[zi, c], self.z, self.y)
 
-    def beside(self, zi, c, to_z):
-        return self.copy(zi, 1 - self.y, c, self.x_s.at[c], self.x_r.at[c], to_z, self.y)
+    def beside(self, k, zi, c, to_z):
+        return self.copy(zi, 1 - self.y, c, self.x_s.at[k, c], self.x_r.at[k, c], to_z, self.y)
 
     def sidesteps(self, c):
-        return 1 <= c and not self.plain(c)
-
-    def plain(self, c):
-        return c == self.chunks - 1
+        middle = jnp.logical_not(self.at_end)
+        cases = []
+        if c in END_FAR:
+            cases.append((self.at_end, 0, self.far, self.inner, self.last - self.outer))
+        if c in END_OWN:
+            cases.append((self.at_end, 1, self.z, self.inner, self.outer))
+        sent, landed = [(p, k, zi, to) for p, k, zi, to, _ in cases], [(middle, k, zi) for _, k, _, _, zi in cases]
+        if c in MID_OWN:
+            sent += [(middle, 2, self.z, self.outer), (middle, 3, self.z, self.far)]
+            landed += [(self.at_end, 2, self.inner), (middle, 3, self.far)]
+        return sent, landed
 
     def crosses(self, zi, c):
         gap = jnp.abs(self.z - zi)
-        near = gap < self.last
-        if self.sidesteps(c):
-            near = near & (gap != 1)
-        if self.plain(c):
-            return (gap >= 0)
-        return jnp.where(self.at_end, near, gap == 1)
+        own_end, own_middle, far_end = c not in END_OWN, c not in MID_OWN, c not in END_FAR
+        from_end = jnp.where(gap == 2, far_end, own_end)
+        at_middle = jnp.where((zi == 0) | (zi == self.last), from_end, own_middle)
+        at_end = jnp.where(gap == 0, own_end, jnp.where(gap == 1, own_middle, jnp.where(gap == 2, True, far_end)))
+        return jnp.where(self.at_end, at_end, at_middle)
 
     def goes_up(self, s):
         return (self.z - s >= 0) & (self.z < self.last)
@@ -170,15 +179,16 @@
         def _():
             self.across(self.z, c).start()
 
+    def start_beside(self, c, kinds):
+        for condition, k, zi, to_z in self.sidesteps(c)[0]:
+            if k in kinds:
+                @pl.when(condition)
+                def _():
+                    self.beside(k, zi, c, to_z).start()
+
     def start_far(self, c):
-        if self.plain(c):
+        if c not in END_FAR:
             self.across(self.far, c).start()
-        else:
-            self.beside(self.far, c, self.inner).start()
-
-    def start_beside(self, c):
-        if self.sidesteps(c):
-            self.beside(self.z, c, self.outer).start()
 
     def hand_on(self, zi, c):
         @pl.when(self.crosses(zi, c))
@@ -206,22 +216,18 @@
                         def _():
                             self.down(s, c).start()
                     self.hand_on(z + s, c)
+            if s == 1:
+                for c in range(self.chunks):
+                    self.start_beside(c, (2, 3))
         for c in range(self.chunks):
             for zi in range(depth):
                 @pl.when(self.crosses(zi, c))
                 def _():
                     self.from_across(zi, c).wait_recv()
-            if not self.plain(c):
-                @pl.when(jnp.logical_not(self.at_end))
+            for condition, k, zi in self.sidesteps(c)[1]:
+                @pl.when(condition)
                 def _():
-                    self.from_beside(self.last - self.outer, c).wait_recv()
-            if self.sidesteps(c):
-                @pl.when(self.at_end)
-                def _():
-                    self.from_beside(self.inner, c).wait_recv()
-
-    def from_beside(self, zi, c):
-        return self.copy(zi, 1 - self.y, c, self.x_s.at[c], self.x_r.at[c], self.z, self.y)
+                    self.beside(k, zi, c, self.z).wait_recv()
 
     def finish(self):
         for c in range(self.chunks):
@@ -237,19 +243,15 @@
                 @pl.when(self.crosses(zi, c))
                 def _():
                     self.across(zi, c).wait_send()
-            if not self.plain(c):
-                @pl.when(self.at_end)
+            for condition, k, zi, to_z in self.sidesteps(c)[0]:
+                @pl.when(condition)
                 def _():
-                    self.beside(self.far, c, self.inner).wait_send()
-            if self.sidesteps(c):
-                @pl.when(jnp.logical_not(self.at_end))
-                def _():
-                    self.beside(self.z, c, self.outer).wait_send()
+                    self.beside(k, zi, c, to_z).wait_send()
 
 
 def gather_sems(depth, chunks):
     dma = pltpu.SemaphoreType.DMA
-    return [dma((depth - 1, chunks))] * 4 + [dma((depth, chunks))] * 2 + [dma((chunks,))] * 2
+    return [dma((depth - 1, chunks))] * 4 + [dma((depth, chunks))] * 2 + [dma((4, chunks))] * 2
 
 
 def kernel(
@@ -260,7 +262,7 @@
     saved, cots, cotx, factors, weights, first, second, moment, moment_new, mapped, terms, crossed, staged, landed,
     smalls, swapped, squares, early, ahead,
     load_sem, fz_s, fz_r, fy_s, fy_r, pair_s, pair_r, cot_s, cot_r, mom_s, mom_r, new_s, new_r, fx_s, fx_r, sx_s, sx_r,
-    wy_s, wy_r, wz_s, wz_r, ty_s, ty_r, tz_s, tz_r, sz_s, sz_r, sy_s, sy_r, norm_s, norm_r, *gather_refs,
+    vy_s, vy_r, wy_s, wy_r, wz_s, wz_r, ty_s, ty_r, tz_s, tz_r, sz_s, sz_r, sy_s, sy_r, norm_s, norm_r, *gather_refs,
 ):
     me, tp = lax.axis_index("fs"), lax.axis_index("tp")
     z, y = me // 2, me % 2
@@ -348,26 +350,27 @@
     part_of = lambda c: pl.ds(c * half, half)
 
     def early_cross(o, c):
-        return send(weights.at[matrix[o], part_of(c)], early.at[0, o, part_of(c)], wy_s.at[o, c], wy_r.at[o, c], beside, tp)
+        return send(weights.at[matrix[o], part_of(c)], early.at[2, o, part_of(c)], wy_s.at[o, c], wy_r.at[o, c], beside, tp)
 
     def early_far(o, c):
         return send(
             weights.at[matrix[o], part_of(c)], early.at[0, o, part_of(c)], wz_s.at[o, c], wz_r.at[o, c], far * 2 + y, tp
         )
 
-    def far_cross(o, c):
-        return send(early.at[0, o, part_of(c)], early.at[1, o, part_of(c)], wy_s.at[o, c], wy_r.at[o, c], beside, tp)
-
-    def early_start(o, c):
+    def far_cross(c):
+        return send(early.at[0, 0, part_of(c)], early.at[1, 0, part_of(c)], vy_s.at[c], vy_r.at[c], beside, tp)
+
+    def bulk_across(i):
         @pl.when(middle)
         def _():
-            early_cross(o, c).start()
-
-    def far_start(o, c):
+            for c in MID_OWN[i : i + 1]:
+                early_cross(c // 2, c % 2).start()
+
         @pl.when(at_end)
         def _():
-            early_far(o, c).wait_recv()
-            far_cross(o, c).start()
+            for c in END_FAR[i : i + 1]:
+                early_far(0, c).wait_recv()
+                far_cross(c).start()
 
     loads[4].wait()
 
@@ -400,9 +403,10 @@
 
     @pl.when(at_end)
     def _():
-        for o in range(2):
-            for c in range(2):
-                early_far(o, c).start()
+        for c in END_OWN:
+            early_cross(c // 2, c % 2).start()
+        for o, c in ((0, 0), (0, 1), (1, 0)):
+            early_far(o, c).start()
 
     map_handed(third * 2 + y)
     map_handed(beside)
@@ -419,24 +423,25 @@
     ]
     for copy in moment_swap:
         copy.start()
-    needed = (jnp.where(at_end, far * 2 + y, beside), jnp.where(at_end, far * 2 + 1 - y, beside))
-
-    def factor_swap(i, m):
-        ref = factors.at[m, needed[i]]
+
+    def factor_swap(m, i=0):
+        ref = factors.at[m, jnp.where(at_end, far * 2 + y, beside) if i == 0 else beside]
         return send(ref, ref, fx_s.at[i], fx_r.at[i], me, opposite)
 
     map_handed(far_one * 2 + 1 - y)
 
-    def term_cross(s, zi):
-        return send(terms.at[s, zi * 2 + 1 - y], crossed.at[s, zi], ty_s.at[s, zi], ty_r.at[s, zi], beside, tp)
-
-    def term_along(s, zi):
-        return send(staged.at[s, zi], landed.at[s, z], tz_s.at[s, zi], tz_r.at[s, z], zi * 2 + y, tp)
-
-    def term_from(s, zi):
-        return send(staged.at[s, z], landed.at[s, zi], tz_s.at[s, z], tz_r.at[s, zi], me, tp)
-
-    order = [k % depth for k in range(1, depth + 1)]
+    def term_cross(t):
+        return send(terms.at[t, 1 - y], crossed.at[t], ty_s.at[t], ty_r.at[t], beside, tp)
+
+    def term_along(t, zi):
+        return send(staged.at[t, zi], landed.at[t, z], tz_s.at[t, zi], tz_r.at[t, z], zi * 2 + y, tp)
+
+    def term_from(t, zi):
+        return send(staged.at[t, z], landed.at[t, zi], tz_s.at[t, z], tz_r.at[t, zi], me, tp)
+
+    others = range(1, depth)
+    piece = slim // 2
+    chunks = [(s, q) for s in range(2) for q in range(2)]
     high, rest = parts_of(mapped[...].T)
     for s in range(2):
         if s == 0:
@@ -444,78 +449,84 @@
         else:
             cot_swap.wait_recv()
             cot = cotx[...]
-        term = dot(high, cot) + dot(rest, cot)
-        terms[s] = term.reshape(n, slim, term.shape[1])
-        for k in order:
-            term_cross(s, (z + k) % depth).start()
-    factor_swap(0, mine).start()
+        term = (dot(high, cot) + dot(rest, cot)).reshape(depth, 2, 2, piece, cot.shape[1])
+        for q in range(2):
+            for column in range(2):
+                terms[2 * s + q, column] = term[:, column, q]
+            term_cross(2 * s + q).start()
+    factor_swap(mine).start()
 
     @pl.when(at_end)
     def _():
-        factor_swap(1, mine).start()
-
-    for s in range(2):
-        for k in order:
-            zi = (z + k) % depth
-            term_cross(s, zi).wait_recv()
-            staged[s, zi] = terms[s, zi * 2 + y] + crossed[s, zi]
-            if k:
-                term_along(s, zi).start()
-    early_start(0, 0)
-    far_start(0, 0)
-
-    def small_along(s, zi):
-        ref = smalls.at[s, me]
-        return send(ref, ref, sz_s.at[s, zi], sz_r.at[s, z], zi * 2 + y, tp)
-
-    def small_from(s, zi):
-        ref = smalls.at[s, zi * 2 + y]
-        return send(ref, ref, sz_s.at[s, zi], sz_r.at[s, zi], me, tp)
-
-    def small_cross(s, zi, column):
-        ref = smalls.at[s, zi * 2 + column]
-        return send(ref, ref, sy_s.at[s, zi], sy_r.at[s, zi], beside, tp)
-
-    def small_swap(block):
-        return send(smalls.at[1, block], swapped.at[block], sx_s.at[block], sx_r.at[block], me, opposite)
+        factor_swap(mine, 1).start()
+
+    for t in range(4):
+        term_cross(t).wait_recv()
+        staged[t] = terms[t, y] + crossed[t]
+        for k in others:
+            term_along(t, (z + k) % depth).start()
+    bulk_across(0)
+
+    def small_piece(t, block):
+        return smalls.at[t // 2, block, pl.ds(t % 2 * piece, piece)]
+
+    def small_along(t, zi):
+        ref = small_piece(t, me)
+        return send(ref, ref, sz_s.at[t, zi], sz_r.at[t, z], zi * 2 + y, tp)
+
+    def small_from(t, zi):
+        ref = small_piece(t, zi * 2 + y)
+        return send(ref, ref, sz_s.at[t, zi], sz_r.at[t, zi], me, tp)
+
+    def small_cross(t, zi, column):
+        ref = small_piece(t, zi * 2 + column)
+        return send(ref, ref, sy_s.at[t, zi], sy_r.at[t, zi], beside, tp)
+
+    def small_swap(t, block):
+        return send(
+            small_piece(t, block), swapped.at[block, pl.ds(t % 2 * piece, piece)],
+            sx_s.at[t % 2, block], sx_r.at[t % 2, block], me, opposite,
+        )
 
     def new_swap(i):
         return send(moment_new.at[i], (first_new, second_new)[i].at[mine], new_s.at[i], new_r.at[i], me, opposite)
 
-    for s in range(2):
-        here = staged[s, z]
-        for k in range(1, depth):
-            term_from(s, (z + k) % depth).wait_recv()
-            here = here + landed[s, (z + k) % depth]
+    for t, (s, q) in enumerate(chunks):
+        part = pl.ds(q * piece, piece)
+        here = staged[t, z]
+        for k in others:
+            term_from(t, (z + k) % depth).wait_recv()
+            here = here + landed[t, (z + k) % depth]
         if s == 0:
-            old_first, old_second = first[mine], second[mine]
+            old_first, old_second = first[mine, part], second[mine, part]
         else:
-            for copy in moment_swap:
-                copy.wait_recv()
-            old_first, old_second = moment[0], moment[1]
+            if q == 0:
+                for copy in moment_swap:
+                    copy.wait_recv()
+            old_first, old_second = moment[0, part], moment[1, part]
         new_first = 0.8 * old_first + 0.2 * here
         new_second = 0.9 * old_second + 0.1 * here * here
-        smalls[s, me] = new_first / (jnp.sqrt(new_second) + 1e-08)
-        for k in range(1, depth):
-            small_along(s, (z + k) % depth).start()
-        small_cross(s, z, y).start()
+        smalls[s, me, part] = new_first / (jnp.sqrt(new_second) + 1e-08)
+        for k in others:
+            small_along(t, (z + k) % depth).start()
+        small_cross(t, z, y).start()
         if s == 0:
-            first_new[mine] = new_first
-            second_new[mine] = new_second
+            first_new[mine, part] = new_first
+            second_new[mine, part] = new_second
         else:
-            small_swap(me).start()
-            moment_new[0] = new_first
-            moment_new[1] = new_second
-    for s in range(2):
-        for k in range(1, depth):
+            small_swap(t, me).start()
+            moment_new[0, part] = new_first
+            moment_new[1, part] = new_second
+    for t, (s, q) in enumerate(chunks):
+        for k in others:
             zi = (z + k) % depth
-            small_from(s, zi).wait_recv()
-            small_cross(s, zi, y).start()
+            small_from(t, zi).wait_recv()
+            small_cross(t, zi, y).start()
             if s == 1:
-                small_swap(zi * 2 + y).start()
-    for o, c in ((0, 1), (1, 0)):
-        early_start(o, c)
-        far_start(o, c)
+                small_swap(t, zi * 2 + y).start()
+    @pl.when(at_end)
+    def _():
+        early_far(1, 1).start()
 
     def send_square(k):
         return send(squares.at[tp], squares.at[tp], norm_s.at[k], norm_r.at[k], me, (tp + k) % tps)
@@ -531,11 +542,14 @@
     columns = smalls.shape[3]
     total = None
     for s in range(2):
-        for k in range(depth):
-            zi = (z + k) % depth
-            small_cross(s, zi, 1 - y).wait_recv()
-            if s == 1:
-                small_swap(zi * 2 + 1 - y).start()
+        for t in (2 * s, 2 * s + 1):
+            for k in range(depth):
+                zi = (z + k) % depth
+                small_cross(t, zi, 1 - y).wait_recv()
+                if s == 1:
+                    small_swap(t, zi * 2 + 1 - y).start()
+        if s == 0:
+            bulk_across(1)
         pieces = parts_of(smalls[s].reshape(n * slim, columns))
         for block in range(n):
             full = full_of(mine, block, pieces)
@@ -554,13 +568,21 @@
 
     late = Late((z, y, tp, depth), 4, chunk_ref, gather_refs)
 
-    def fill_full(m, pieces):
+    def fill_full(m, pieces, o):
         update[m] = full_of(m, me, pieces)
-        ahead[0] = full_of(m, needed[0], pieces)
 
         @pl.when(at_end)
         def _():
-            ahead[1] = full_of(m, needed[1], pieces)
+            ahead[0] = full_of(m, far * 2 + y, pieces)
+            if o == 0:
+                ahead[1] = full_of(m, far * 2 + 1 - y, pieces)
+            if any(c // 2 == o for c in END_OWN):
+                ahead[2] = full_of(m, beside, pieces)
+
+        if any(c // 2 == o for c in MID_OWN):
+            @pl.when(middle)
+            def _():
+                ahead[2] = full_of(m, beside, pieces)
 
     def root_of(m):
         mean = jnp.sum(squares[2 * m] + squares[2 * m + 1], keepdims=True) / entries
@@ -569,20 +591,21 @@
     for o in range(2):
         m = matrix[o]
         if o == 0:
-            fill_full(m, own_pieces)
+            fill_full(m, own_pieces, o)
             recv_square((tp + tps - partner) % tps).wait_recv()
         else:
+            for block in range(n):
+                for t in (2, 3):
+                    small_swap(t, block).wait_recv()
+            factor_swap(other).wait_recv()
+
+            @pl.when(at_end)
+            def _():
+                factor_swap(other, 1).wait_recv()
+
+            fill_full(m, parts_of(swapped[...].reshape(n * slim, columns)), o)
             for k in range(2):
                 recv_square((tp + tps - other * 2 - k) % tps).wait_recv()
-            for block in range(n):
-                small_swap(block).wait_recv()
-            factor_swap(0, other).wait_recv()
-
-            @pl.when(at_end)
-            def _():
-                factor_swap(1, other).wait_recv()
-
-            fill_full(m, parts_of(swapped[...].reshape(n * slim, columns)))
         root = root_of(m)
         new_update = update[m] / root
         new_weight = weights[m] - 0.02 * new_update
@@ -595,27 +618,35 @@
         def fill(block, c, slot):
             copies[m, block, part_of(c)] = (early[slot, o, part_of(c)] - 0.02 * (ahead[slot, part_of(c)] / root)).astype(BF16)
 
-        halves = [c for c in range(2) if not late.plain(2 * o + c)]
+        def fill_beside(c):
+            early_cross(o, c % 2).wait_recv()
+            fill(beside, c % 2, 2)
 
         @pl.when(middle)
         def _():
-            for c in halves:
-                early_cross(o, c).wait_recv()
-                fill(beside, c, 0)
-                late.start_beside(2 * o + c)
+            for c in MID_OWN:
+                if c // 2 == o:
+                    fill_beside(c)
 
         @pl.when(at_end)
         def _():
-            for c in range(2):
-                if c in halves:
-                    far_cross(o, c).wait_recv()
+            for c in range(2 * o, 2 * o + 2):
+                if c in END_FAR:
+                    far_cross(c).wait_recv()
                     fill(far * 2 + 1 - y, c, 1)
+                    late.start_beside(c, (0,))
                 else:
-                    early_far(o, c).wait_recv()
+                    if o == 1:
+                        early_far(o, c % 2).wait_recv()
+                    fill(far * 2 + y, c % 2, 0)
+                    late.start_far(c)
+            for c in END_OWN:
+                if c // 2 == o:
+                    fill_beside(c)
+                    late.start_beside(c, (1,))
+            for c in END_FAR:
+                if c // 2 == o:
                     fill(far * 2 + y, c, 0)
-                late.start_far(2 * o + c)
-            for c in halves:
-                fill(far * 2 + y, c, 0)
 
     late.relay()
     for i in range(2):
@@ -623,18 +654,25 @@
 
     @pl.when(middle)
     def _():
-        for o, c in ((0, 0), (0, 1), (1, 0)):
-            early_cross(o, c).wait_send()
+        for c in MID_OWN:
+            early_cross(c // 2, c % 2).wait_send()
 
     @pl.when(at_end)
     def _():
-        for o, c in ((0, 0), (0, 1), (1, 0), (1, 1)):
-            if not late.plain(2 * o + c):
-                far_cross(o, c).wait_send()
-            early_far(o, c).wait_send()
-        factor_swap(1, mine).wait_send()
-
-    factor_swap(0, mine).wait_send()
+        for c in END_OWN:
+            early_cross(c // 2, c % 2).wait_send()
+        for c in END_FAR:
+            far_cross(c).wait_send()
+        for o in range(2):
+            for c in range(2):
+                early_far(o, c).wait_send()
+
+    factor_swap(mine).wait_send()
+
+    @pl.when(at_end)
+    def _():
+        factor_swap(mine, 1).wait_send()
+
     late.finish()
     cot_swap.wait_send()
     for i in range(2):
@@ -643,18 +681,20 @@
     for k in range(1, n):
         hand((me + k) % n).wait_send()
     for k in range(n):
-        small_swap(k).wait_send()
+        for t in (2, 3):
+            small_swap(t, k).wait_send()
     for k in range(depth):
         zi = (z + k) % depth
         factor_cross(zi, y).wait_send()
         if k:
             factor_along(zi).wait_send()
-        for s in range(2):
-            term_cross(s, zi).wait_send()
-            small_cross(s, zi, y).wait_send()
+        for t in range(4):
+            if not k:
+                term_cross(t).wait_send()
+            small_cross(t, zi, y).wait_send()
             if k:
-                term_along(s, zi).wait_send()
-                small_along(s, zi).wait_send()
+                term_along(t, zi).wait_send()
+                small_along(t, zi).wait_send()
     for k in range(1, tps):
         send_square(k).wait_send()
 
@@ -700,21 +740,23 @@
             pltpu.VMEM((2, rows, columns), F32),
             *[pltpu.VMEM((2, slim, columns), F32)] * 4,
             pltpu.VMEM((tokens, rank), F32),
-            pltpu.VMEM((2, n, slim, columns), F32),
-            *[pltpu.VMEM((2, depth, slim, columns), F32)] * 3,
+            pltpu.VMEM((4, 2, depth, slim // 2, columns), F32),
+            *[pltpu.VMEM((4, depth, slim // 2, columns), F32)] * 3,
             pltpu.VMEM((2, n, slim, columns), F32),
             pltpu.VMEM((n, slim, columns), F32),
             pltpu.VMEM((tps, 8, columns), F32),
-            pltpu.VMEM((2, 2, rows, columns), F32),
-            pltpu.VMEM((2, rows, columns), F32),
+            pltpu.VMEM((3, 2, rows, columns), F32),
+            pltpu.VMEM((3, rows, columns), F32),
             dma((11,)),
             *[dma((depth,))] * 4,
             dma((n,)), dma((n,)),
             dma, dma,
             *[dma((2,))] * 6,
-            dma((n,)), dma((n,)),
+            dma((2, n)), dma((2, n)),
+            dma((2,)), dma((2,)),
             *[dma((2, 2))] * 4,
-            *[dma((2, depth))] * 8,
+            dma((4,)), dma((4,)),
+            *[dma((4, depth))] * 6,
             dma((tps,)), dma((tps,)),
             *gather_sems(depth, 4),
         ],
@@ -737,7 +779,7 @@
 def on_device(saved_input, cot_inproj, cot_outproj, factor_inproj, *others):
     n, tps = lax.axis_size("fs"), lax.axis_size("tp")
     rows, rank = factor_inproj.shape
-    if n == 8 and tps == 4 and rank % (8 * n) == 0 and rows % 128 == 0 and cot_inproj.shape[1] % 128 == 0:
+    if n == 8 and tps == 4 and rank % (16 * n) == 0 and rows % 128 == 0 and cot_inproj.shape[1] % 128 == 0:
         return kernel_form(n, tps, saved_input, cot_inproj, cot_outproj, factor_inproj, *others)
     return plain_form(saved_input, cot_inproj, cot_outproj, factor_inproj, *others)
 

time: 66.9 us -> 63.6 us (0.951)
  Pallas kernels: 66.1 us -> 62.8 us
    pallas_call x1, Pallas kernels: 64.4 us -> 61 us  [kernel_form(): pl.pallas_call(functools.partial(kernel, n, tps, entries), out_shape=(sha...]
where the time goes in v4:
time: 63.6 us; the launch traced here: 63.4 us
  Pallas kernels  62.8 us (99%)
  between operations  0.65 us (1%)
    pallas_call x1, Pallas kernels, kernel_form(): pl.pallas_call(functools.partial(kernel, n, tps, entries), out_shape=(sha...  61 us
    pallas_call x1, Pallas kernels, kernel_form(): pl.pallas_call(write_kernel, out_shape=(*[shape((rows, columns), F32)] *...  1.77 us

profile of v4, /device:TPU:0, one launch (start us, length us, event | category | flops | bytes accessed | tf_op | source)
XLA Modules:
  0.0 63.4 jit_solution(12893935008860507617)
XLA Ops:
  0.6 61.0 %shard_map.186 = (f32[2,256,256]{2,1,0:T(8,128)S(1)}, f32[2,256,256]{2,1,0:T(8,128)S(1)}, bf16[2,8,256,256]{3,2,1,0:T(8,128)(2,1)S(1)}, f32[2,32,256]{2,1,0:T(8,128)S(1)}, f32[2,32,256]{2,1,0:T(8,128)S(1)}) custom-call(bf16[768,2048]{1,0:T(8,128)(2,1)} %saved_hbm.1, bf16[768,256]{1,0:T(8,128)(2,1)} %cot_in_hbm.1, bf16[768,256]{1,0:T(8,128)(2,1)} %cot_out_hbm.1, ...), custom_call_target="tpu_custom_call" | custom-call | tf_op jit(solution)/shard_map/pallas_call | solution.py:726
  61.6 1.8 %shard_map.187 = (f32[256,256]{1,0:T(8,128)}, f32[256,256]{1,0:T(8,128)}, f32[256,256]{1,0:T(8,128)}, f32[256,256]{1,0:T(8,128)}, bf16[2048,256]{1,0:T(8,128)(2,...) custom-call(f32[2,256,256]{2,1,0:T(8,128)S(1)} %get-tuple-element.15, ...), custom_call_target="tpu_custom_call" | custom-call | tf_op jit(solution)/shard_map/pallas_call | solution.py:767
